TPU v7x, 32 devices: a whole 2x2x4 slice. The times are simulated.
32 devices in a mesh: sp: 16 (over z, y, x), tp: 2 (over core).
Axes of the slice: x: 2, y: 2, z: 4, core: 2. Of those that a mesh axis runs over, the one named last changes fastest.
Arguments:
- value_in: bfloat16 [4096, 2048], P('sp', 'tp'), may hold values from -25 to 25, as said below
- gate_in: bfloat16 [4096, 2048], P('sp', 'tp'), may hold values from -6 to 6
- taps: float32 [31, 2048], P(None, 'tp'), may hold values from -1 to 1
- gain: float32 [2048], P('tp'), may hold values from 0.1 to 1.9
- shift: float32 [2048], P('tp'), may hold values from -3 to 3
- w_out: bfloat16 [2048, 2048], P('tp'), may hold values from -0.125 to 0.125
- grad_out: bfloat16 [4096, 2048], P('sp'), may hold values from -6 to 6
Outputs:
- d_value: bfloat16 [4096, 2048], P('sp', 'tp')
- d_gate: bfloat16 [4096, 2048], P('sp', 'tp')
- d_taps: float32 [31, 2048], P(None, 'tp')
- d_gain: float32 [2048], P('tp')
- d_shift: float32 [2048], P('tp')
Inputs may be any that keep to these rules, and one draw needn't show every extreme that they name: `value_in`: channel blocks of different magnitude.
All inputs are finite; a program needn't handle non-finite values.
Results may differ from a plain program's by a relative error of at most 0.007.
Values may be sent and summed in bfloat16 or wider, within the bound.
No kernel may reach another device: no remote copies, remote signals or barrier semaphores. Data moves between devices by JAX's collectives and lax.ppermute only.
A program may use at most 64 MiB of HBM per device.

v0:
```python
import functools
import math

import jax
import jax.numpy as jnp
from jax import lax
from jax.experimental import pallas as pl
from jax.experimental.pallas import tpu as pltpu
from jax.sharding import PartitionSpec as P


EPS = 1e-05
LANES = 128
F32 = jnp.float32
BF16 = jnp.bfloat16
VMEM = pl.BlockSpec(memory_space=pltpu.VMEM)
HBM = pl.BlockSpec(memory_space=pltpu.HBM)


def up(value, step):
    return -(-value // step) * step


def in_hbm(*arrays):
    return [pltpu.with_memory_space_constraint(array, pltpu.HBM) for array in arrays]


def call(body, outs, args, aliases=None, flops=0, specs=None, out_specs=None, scratch=()):
    return pl.pallas_call(
        body,
        out_shape=[jax.ShapeDtypeStruct(shape, dtype) for shape, dtype in outs],
        in_specs=specs if specs else [VMEM] * len(args),
        out_specs=out_specs if out_specs else [VMEM] * len(outs),
        input_output_aliases=aliases or {},
        scratch_shapes=list(scratch),
        compiler_params=pltpu.CompilerParams(vmem_limit_bytes=16 * 2**20),
        cost_estimate=pl.CostEstimate(flops=flops, bytes_accessed=0, transcendentals=0),
    )(*args)


def parity():
    return lax.rem(lax.axis_index("sp"), 2)


def gate_rows(value, gate):
    sig = jax.nn.sigmoid(gate.astype(F32))
    return (value.astype(F32) * sig).astype(BF16)


def edge_rows(pad, value_hbm, gate_hbm, send_even, send_odd, value, gate, sems):
    rows = value_hbm.shape[0]
    odd = parity()
    copies = []
    for at, top in enumerate((odd, 1 - odd)):
        span = pl.ds(pl.multiple_of((1 - top) * (rows - pad), pad), pad)
        copies += [
            pltpu.make_async_copy(value_hbm.at[span, :], value.at[at], sems.at[2 * at]),
            pltpu.make_async_copy(gate_hbm.at[span, :], gate.at[at], sems.at[2 * at + 1]),
        ]
    for copy in copies:
        copy.start()
    for copy in copies:
        copy.wait()
    send_even[...] = gate_rows(value[0], gate[0])
    send_odd[...] = gate_rows(value[1], gate[1])


def gate_and_mix(pad, tile, value, gate, grads, w, gated, mix):
    rows, channels = value.shape
    for index in range(channels // tile):
        if index * tile // LANES < mix.shape[0]:
            mix_rows(tile, index, 0, grads, w, mix)
        for part in range(tile // LANES):
            block = index * (tile // LANES) + part
            lanes = slice(block * LANES, (block + 1) * LANES)
            gated[block, pad : pad + rows, :] = gate_rows(value[:, lanes], gate[:, lanes]).astype(F32)


def mix_rows(tile, index, first, grads, w, mix):
    mixed = lax.dot_general(
        grads[...],
        w[index * tile : (index + 1) * tile, :],
        (((1,), (1,)), ((), ())),
        preferred_element_type=F32,
    )
    for part in range(tile // LANES):
        block = index * (tile // LANES) + part - first
        mix[block] = mixed[:, part * LANES : (part + 1) * LANES]


def mix_rest(tile, first, grads, w, mix):
    for index in range(first * LANES // tile, w.shape[0] // tile):
        mix_rows(tile, index, first, grads, w, mix)


def conv_rows(taps, source, block, lanes, first, count, shift):
    total = jnp.zeros((count, LANES), F32)
    for tap in range(taps.shape[0]):
        total = total + taps[pl.ds(tap, 1), lanes] * source[block, pl.ds(first + tap + shift, count), :]
    return total


def pieces(first, last, most):
    count = -(-(last - first) // most)
    size = up(-(-(last - first) // count), 8)
    return [(at, min(size, last - at)) for at in range(first, last, size)]


def row_sums(conv, part, first, last):
    def sums(chunk, carry):
        rows = pl.ds(pl.multiple_of(first + chunk * 16, 16), 16)
        total = jnp.zeros((16, LANES), F32)
        squares = jnp.zeros((16, LANES), F32)
        for block in range(conv.shape[0]):
            value = conv[block, rows, :]
            total = total + value
            squares = squares + value * value
        part[0, rows, :] = total
        part[1, rows, :] = squares
        return carry

    lax.fori_loop(0, (last - first) // 16, sums, 0)


def conv_inner(pad, gated, taps, out, part):
    blocks, height, _ = out.shape
    shift = pad - taps.shape[0] // 2

    def body(block, carry):
        lanes = pl.ds(pl.multiple_of(block * LANES, LANES), LANES)
        for at, count in pieces(pad, height - pad, 56):
            out[block, at : at + count, :] = conv_rows(taps, gated, block, lanes, at, count, shift)
        return carry

    lax.fori_loop(0, blocks, body, 0)
    row_sums(out, part, pad, height - pad)


def fill_halo(pad, from_even, from_odd, frame, block, lanes):
    rows = frame.shape[1] - 2 * pad
    odd = parity() == 1
    even_rows = from_even[:, lanes].astype(F32)
    odd_rows = from_odd[:, lanes].astype(F32)
    frame[block, :pad, :] = jnp.where(odd, even_rows, odd_rows)
    frame[block, pad + rows :, :] = jnp.where(odd, odd_rows, even_rows)


def thirds(x):
    high = x.astype(BF16).astype(F32)
    middle = (x - high).astype(BF16).astype(F32)
    return high, middle, (x - high) - middle


def lane_sums(first, second):
    stacked = jnp.concatenate([first[...], second[...]], 0)
    split = jnp.concatenate(thirds(stacked), 1).astype(BF16)
    ones = jnp.ones((16, split.shape[1]), BF16)
    return lax.dot_general(
        ones, split, (((1,), (1,)), ((), ())), preferred_element_type=F32
    )[0:1]


def spread(lines):
    rows = [row for line in lines for row in thirds(line)]
    rows += [jnp.zeros_like(lines[0])] * (16 - len(rows))
    shape = (16, len(lines) * LANES)
    part = lax.broadcasted_iota(jnp.int32, shape, 0)
    block = lax.broadcasted_iota(jnp.int32, shape, 1) // LANES
    chosen = jnp.logical_and(part >= 3 * block, part < 3 * block + 3)
    return lax.dot_general(
        jnp.concatenate(rows, 0).astype(BF16),
        chosen.astype(F32).astype(BF16),
        (((0,), (0,)), ((), ())),
        preferred_element_type=F32,
    )


def conv_edges(pad, from_even, from_odd, taps, gated_in, conv_in, part_in, gated, conv, part, stats):
    blocks, height, _ = conv.shape
    shift = pad - taps.shape[0] // 2

    def fill(block, carry):
        lanes = pl.ds(pl.multiple_of(block * LANES, LANES), LANES)
        fill_halo(pad, from_even, from_odd, gated, block, lanes)
        for at in (0, height - pad):
            conv[block, at : at + pad, :] = conv_rows(taps, gated, block, lanes, at, pad, shift)
        return carry

    lax.fori_loop(0, blocks, fill, 0)
    row_sums(conv, part, 0, pad)
    row_sums(conv, part, height - pad, height)
    stats[...] = lane_sums(part[0], part[1])


def moments(mine, other, width):
    total = (mine[...] + other[...]) / width
    rows = total.shape[1] // 2
    mean = total[:, :rows]
    var = total[:, rows:] - mean * mean
    return mean, lax.rsqrt(var + EPS)


def norm_back(
    width,
    at,
    conv,
    mix_low,
    mix_high,
    stats,
    stats_other,
    gain,
    shift,
    normed,
    grad,
    second,
    sums,
    part,
    line,
):
    blocks, height, _ = normed.shape
    half = mix_low.shape[0]
    mean, inv = moments(stats, stats_other, width)
    line[...] = spread([mean[:, at : at + height], inv[:, at : at + height]])

    def body(chunk, carry):
        rows = pl.ds(pl.multiple_of(chunk * 16, 16), 16)
        whole = pl.ds(pl.multiple_of(at + chunk * 16, 16), 16)
        mean_rows = line[rows, :LANES]
        inv_rows = line[rows, LANES:]
        first = jnp.zeros((16, LANES), F32)
        other = jnp.zeros((16, LANES), F32)
        kept = []
        for block in range(blocks):
            lanes = slice(block * LANES, (block + 1) * LANES)
            norm = (conv[block, whole, :] - mean_rows) * inv_rows
            mixed = mix_low[block, whole, :] if block < half else mix_high[block - half, whole, :]
            gain_row = gain[:, lanes]
            pre = norm * gain_row + shift[:, lanes]
            sig = jax.nn.sigmoid(pre)
            grad_pre = mixed * sig * (1.0 + pre * (1.0 - sig))
            grad_norm = grad_pre * gain_row
            normed[block, rows, :] = norm
            grad[block, rows, :] = grad_norm
            first = first + grad_norm
            other = other + grad_norm * norm
            product = grad_pre * norm
            kept += [product[:8] + product[8:], grad_pre[:8] + grad_pre[8:]]
        part[0, rows, :] = first
        part[1, rows, :] = other
        return tuple(old + new for old, new in zip(carry, kept))

    zero = tuple(jnp.zeros((8, LANES), F32) for _ in range(2 * blocks))
    totals = lax.fori_loop(0, height // 16, body, zero)
    for block in range(blocks):
        for which in range(2):
            sums[which, block : block + 1, :] = jnp.sum(totals[2 * block + which], 0, keepdims=True)
    second[...] = lane_sums(part[0], part[1])


def tap_sums(
    pad, width, kernel, at, height, normed, grad, stats, stats_other, second, second_other, gated, *refs
):
    blocks, count, _ = normed.shape
    each = up(kernel + 1, 16)
    shift = pad - kernel // 2
    odd = parity() == 1
    final = at + count == height
    if final:
        sums_low, sums_high, _, raw_in, grad_conv, packed, send_odd, line, raw = refs
    else:
        grad_conv, raw, line = refs
    _, inv = moments(stats, stats_other, width)
    total = (second[...] + second_other[...]) / width
    line[...] = spread([inv[:, at : at + count], total[:, :count], total[:, count:]])
    if not final:
        raw[...] = jnp.zeros_like(raw)

    def body(block, carry):
        for low, size in pieces(0, count, 32):
            span = slice(low, low + size)
            grad_conv[block, pad + at + low : pad + at + low + size, :] = line[span, :LANES] * (
                grad[block, span, :]
                - line[span, LANES : 2 * LANES]
                - normed[block, span, :] * line[span, 2 * LANES :]
            )
        base = pl.multiple_of(block * each, each)
        for low in range(0, kernel, 16):
            taps = range(low, min(low + 16, kernel))
            totals = [jnp.zeros((8, LANES), F32) for _ in taps]
            for row in range(at, at + count, 32):
                own = grad_conv[block, pad + row : pad + row + 32, :]
                for index, tap in enumerate(taps):
                    term = own * gated[block, pl.ds(row + tap + shift, 32), :]
                    totals[index] = totals[index] + (
                        (term[0:8] + term[8:16]) + (term[16:24] + term[24:32])
                    )
            for index, tap in enumerate(taps):
                line_sum = jnp.sum(totals[index], 0, keepdims=True)
                if final:
                    line_sum += raw_in[pl.ds(base + tap, 1), :]
                raw[pl.ds(base + tap, 1), :] = line_sum
        if final:
            one = pl.ds(block, 1)
            raw[pl.ds(base + kernel, 1), :] = sums_low[0, one, :] + sums_high[0, one, :]
            top = grad_conv[block, pad : 2 * pad, :].astype(BF16)
            bottom = grad_conv[block, height : height + pad, :].astype(BF16)
            place = pl.multiple_of(block * pad, pad)
            packed[pl.ds(place + raw.shape[0], pad), :] = jnp.where(odd, top, bottom)
            send_odd[pl.ds(place, pad), :] = jnp.where(odd, bottom, top)
        return carry

    if final:
        raw[blocks * each :, :] = raw_in[blocks * each :, :]
    lax.fori_loop(0, blocks, body, 0)
    if final:
        raw[blocks * each : blocks * each + blocks, :] = sums_low[1] + sums_high[1]
        packed[: raw.shape[0]] = raw[...].astype(BF16)


def fill_back(pad, even, later, odd, frame):
    blocks, height, _ = frame.shape
    base = even.shape[0] - blocks * pad
    upper = parity() == 1
    early = lax.axis_index("tp") == 0

    def fill(block, carry):
        place = pl.multiple_of(block * pad, pad)
        even_rows = jnp.where(
            early, even[pl.ds(place + base, pad), :], later[pl.ds(place + base, pad), :]
        ).astype(F32)
        odd_rows = odd[pl.ds(place, pad), :].astype(F32)
        frame[block, :pad, :] = jnp.where(upper, even_rows, odd_rows)
        frame[block, height - pad :, :] = jnp.where(upper, odd_rows, even_rows)
        return carry

    lax.fori_loop(0, blocks, fill, 0)


def conv_back(pad, stage, spans, before, grad_conv, taps, value, gate, *refs):
    blocks = grad_conv.shape[0]
    kernel = taps.shape[0]
    top = pad + kernel // 2
    sems = refs[-1]
    if stage == 2:
        held_value, held_gate = refs[-3:-1]
        even, later, odd = refs[:3]
        old_value, old_gate = refs[3:5]
        frame, d_value, d_gate = refs[7:10]
        fill_back(pad, even, later, odd, frame)
        grad_conv = frame
    elif stage == 1:
        old_value, old_gate = refs[:2]
        held_value, held_gate, d_value, d_gate = refs[2:6]
    else:
        held_value, held_gate = refs[:2]
    copies = []

    def write(held_pair, which):
        base = 0
        for at, count in which:
            for held, out in zip(held_pair, (d_value, d_gate)):
                copy = pltpu.make_async_copy(
                    held.at[pl.ds(base, count), :],
                    out.at[pl.ds(at, count), :],
                    sems.at[len(copies)],
                )
                copy.start()
                copies.append(copy)
            base += count

    if stage:
        write((old_value, old_gate), before)
    base = 0
    for at, count in spans:
        span = slice(base, base + count)
        base += count

        def body(block, carry):
            lanes = pl.ds(pl.multiple_of(block * LANES, LANES), LANES)
            total = jnp.zeros((count, LANES), F32)
            for tap in range(kernel):
                total = total + taps[pl.ds(tap, 1), lanes] * grad_conv[
                    block, pl.ds(at + top - tap, count), :
                ]
            sig = jax.nn.sigmoid(gate[at : at + count, lanes].astype(F32))
            scaled = total * sig
            held_value[span, lanes] = scaled.astype(BF16)
            held_gate[span, lanes] = (
                scaled * value[at : at + count, lanes].astype(F32) * (1.0 - sig)
            ).astype(BF16)
            return carry

        lax.fori_loop(0, blocks, body, 0)
    if stage == 2:
        write((held_value, held_gate), spans)
    for copy in copies:
        copy.wait()


def merge(summed, mine, other, *refs):
    out = refs[-1]
    rows = summed
    out[:rows] = (mine[:rows].astype(F32) + other[:rows].astype(F32)).astype(BF16)
    if out.shape[0] > rows:
        out[rows:] = mine[rows:]


def unpack(scale, kernel, mine, other, d_taps, d_gain, d_shift):
    each = up(kernel + 1, 16)
    blocks = d_gain.shape[0]
    total = (mine[...].astype(F32) + other[...].astype(F32)) * scale
    for block in range(blocks):
        base = block * each
        d_taps[:, block * LANES : (block + 1) * LANES] = total[base : base + kernel]
        d_gain[block : block + 1, :] = total[base + kernel : base + kernel + 1]
    d_shift[...] = total[blocks * each : blocks * each + blocks]


def swap_cores(line):
    assert lax.axis_size("tp") == 2
    return lax.ppermute(line, "tp", [(0, 1), (1, 0)])


def radices(count):
    twos = []
    odds = []
    step = 1
    while (count // step) % 2 == 0:
        twos.append(step)
        step *= 2
    odd = 3
    while step < count:
        while (count // step) % odd == 0:
            odds.append((odd, step))
            step *= odd
        odd += 2
    return twos, odds


def turn(count, radix, step, shift_by):
    pairs = []
    for i in range(count):
        digit = (i // step) % radix
        pairs.append((i, i + ((digit + shift_by) % radix - digit) * step))
    return pairs


def shards(value_in, gate_in, taps, gain, shift, w_out, grad_out):
    kernel, channels = taps.shape
    rows = value_in.shape[0]
    count = lax.axis_size("sp")
    width = channels * lax.axis_size("tp")
    blocks = channels // LANES
    pad = up(kernel // 2 + 1, 16)
    index = lax.axis_index("sp")
    tile = 2 * LANES if channels % (2 * LANES) == 0 else LANES
    each = up(kernel + 1, 16)
    wide = ((blocks, rows + 2 * pad, LANES), F32)
    frame = ((blocks, rows, LANES), F32)
    lines = ((1, 2 * rows), F32)
    send = ((pad, channels), BF16)
    conv_flops = 2 * kernel * rows * channels
    swap_odd = [(i, i + 1) for i in range(1, count - 1, 2)]
    swap_even = [(i, i + 1) for i in range(0, count - 1, 2)]
    swap_odd += [(b, a) for a, b in swap_odd]
    swap_even += [(b, a) for a, b in swap_even]

    send_even, send_odd = call(
        functools.partial(edge_rows, pad),
        [send, send],
        in_hbm(value_in, gate_in),
        specs=[HBM] * 2,
        scratch=[
            pltpu.VMEM((2, pad, channels), BF16),
            pltpu.VMEM((2, pad, channels), BF16),
            pltpu.SemaphoreType.DMA((4,)),
        ],
        flops=2000 * conv_flops,
    )
    from_odd = lax.ppermute(send_odd, "sp", swap_odd)
    from_even = lax.ppermute(send_even, "sp", swap_even)
    low_blocks = channels // tile // 2 * tile // LANES
    high_blocks = blocks - low_blocks
    gated, mix_low = call(
        functools.partial(gate_and_mix, pad, tile),
        [wide, ((low_blocks, rows, LANES), F32)],
        (value_in, gate_in, grad_out, w_out),
        flops=2 * conv_flops,
    )
    conv, part = call(
        functools.partial(conv_inner, pad),
        [frame, ((2, rows, LANES), F32)],
        (gated, taps),
        flops=conv_flops,
    )
    gated, conv, part, stats = call(
        functools.partial(conv_edges, pad),
        [wide, frame, ((2, rows, LANES), F32), lines],
        (from_even, from_odd, taps, gated, conv, part),
        aliases={3: 0, 4: 1, 5: 2},
        flops=conv_flops,
    )
    stats_other = swap_cores(stats)
    (mix_high,) = call(
        functools.partial(mix_rest, tile, low_blocks),
        [((high_blocks, rows, LANES), F32)],
        (grad_out, w_out),
        flops=conv_flops,
    )
    assert count % 2 == 0
    packed_rows = up(blocks * each + blocks, 16)
    height = up(rows // 2, LANES) if rows > LANES else rows
    halves = [(at, min(height, rows - at)) for at in range(0, rows, height)]
    assert len(halves) == 2
    ready = []
    for at, size in halves:
        normed, grad, second, sums = call(
            functools.partial(norm_back, width, at),
            [((blocks, size, LANES), F32)] * 2 + [((1, 2 * size), F32), ((2, blocks, LANES), F32)],
            (conv, mix_low, mix_high, stats, stats_other, gain[None], shift[None]),
            scratch=[pltpu.VMEM((2, size, LANES), F32), pltpu.VMEM((size, 2 * LANES), F32)],
            flops=conv_flops // 2,
        )
        ready.append((normed, grad, stats, stats_other, second, swap_cores(second), gated, sums))
    (at, size), (next_at, next_size) = halves
    grad_conv, raw = call(
        functools.partial(tap_sums, pad, width, kernel, at, rows),
        [wide, ((packed_rows, LANES), F32)],
        ready[0][:-1],
        scratch=[pltpu.VMEM((size, 3 * LANES), F32)],
        flops=conv_flops // 2,
    )
    grad_conv, packed, send_odd = call(
        functools.partial(tap_sums, pad, width, kernel, next_at, rows),
        [wide, ((packed_rows + blocks * pad, LANES), BF16), ((blocks * pad, LANES), BF16)],
        (*ready[1][:-1], ready[0][-1], ready[1][-1], grad_conv, raw),
        aliases={9: 0},
        scratch=[pltpu.VMEM((next_size, 3 * LANES), F32), pltpu.VMEM((packed_rows, LANES), F32)],
        flops=conv_flops // 2,
    )
    twos, odds = radices(count)
    cores = lax.axis_size("tp")
    orders = [twos, twos[1::-1] + twos[:1:-1]]

    def exchange(at, array):
        pairs = []
        for core in range(cores):
            for a, b in turn(count, 2, orders[core % 2][at], 1):
                pairs.append((a * cores + core, b * cores + core))
        return lax.ppermute(array, ("sp", "tp"), pairs)

    def add(mine, other, height, *after):
        return call(
            functools.partial(merge, packed_rows), [((height, LANES), BF16)], (mine, other, *after)
        )[0]

    first = exchange(0, packed)
    grads_odd = lax.ppermute(send_odd, "sp", swap_odd)

    out = ((rows, channels), BF16)
    middle = up(rows // 2, 16)
    spans = (pieces(pad, middle, 64), pieces(middle, rows - pad, 64))
    edges = [(0, pad), (rows - pad, pad)]
    held = [((sum(n for _, n in part), channels), BF16) for part in (*spans, edges)]
    sources = (grad_conv, taps, value_in, gate_in)
    later, mine = first, packed
    if len(twos) > 1:
        mine = add(packed, first, packed.shape[0])
        later = exchange(1, mine)
    old = call(
        functools.partial(conv_back, pad, 0, spans[0], ()),
        [held[0]] * 2,
        sources,
        scratch=[pltpu.SemaphoreType.DMA((1,))],
        flops=conv_flops // 2,
    )
    *held_rows, d_value, d_gate = call(
        functools.partial(conv_back, pad, 1, spans[1], spans[0]),
        [held[1]] * 2 + [out] * 2,
        (*sources, *old),
        out_specs=[VMEM] * 2 + [HBM] * 2,
        scratch=[pltpu.SemaphoreType.DMA((2 * len(spans[0]),))],
        flops=conv_flops // 2,
    )
    _, d_value, d_gate = call(
        functools.partial(conv_back, pad, 2, edges, spans[1]),
        [wide, out, out],
        (*sources, first, later, grads_odd, *held_rows, d_value, d_gate),
        specs=[VMEM] * 9 + [HBM] * 2,
        out_specs=[VMEM] + [HBM] * 2,
        aliases={0: 0, 9: 1, 10: 2},
        scratch=[pltpu.VMEM(*held[2])] * 2
        + [pltpu.SemaphoreType.DMA((2 * len(spans[1]) + 2 * len(edges),))],
        flops=conv_flops // 8,
    )
    ended = {1: [old[0]], 2: [held_rows[0]]}
    other = later
    for at in range(2, len(twos)):
        mine = add(mine, other, packed_rows, *ended.get(at - 1, []))
        other = exchange(at, mine)
    for radix, step in odds:
        mine = add(mine, other, packed_rows)
        digit = (index // step) % radix
        parts = [mine] + [
            lax.ppermute(mine, "sp", turn(count, radix, step, shift_by))
            for shift_by in range(1, radix)
        ]
        total = jnp.zeros(mine.shape, F32)
        for place in range(radix):
            term = parts[0]
            for away in range(1, radix):
                term = jnp.where((digit - away) % radix == place, parts[away], term)
            total = total + term.astype(F32)
        mine = lax.reduce_precision(total, 8, 7).astype(BF16)
        other = jnp.zeros_like(mine)
    mine, other = mine[:packed_rows], other[:packed_rows]
    d_taps, d_gain, d_shift = call(
        functools.partial(unpack, 1.0 / math.sqrt(rows * count), kernel),
        [((kernel, channels), F32), ((blocks, LANES), F32), ((blocks, LANES), F32)],
        (mine, other),
    )
    return (d_value, d_gate, d_taps, d_gain.reshape(channels), d_shift.reshape(channels))


def solution(mesh):
    return jax.shard_map(
        shards,
        mesh=mesh,
        in_specs=(
            P("sp", "tp"),
            P("sp", "tp"),
            P(None, "tp"),
            P("tp"),
            P("tp"),
            P("tp", None),
            P("sp", None),
        ),
        out_specs=(P("sp", "tp"), P("sp", "tp"), P(None, "tp"), P("tp"), P("tp")),
        check_vma=False,
    )
```

profile of v0, /device:TPU:8, one launch (start us, length us, event | category | flops | bytes accessed | tf_op | source)
XLA Modules:
  0.0 44.8 jit_solution(18185706518692887447)
XLA Ops:
  0.7 1.0 %shard_map.110 = (bf16[16,1024]{1,0:T(8,128)(2,1)S(1)}, bf16[16,1024]{1,0:T(8,128)(2,1)S(1)}) custom-call(bf16[256,1024]{1,0:T(8,128)(2,1)} %value.7, bf16[256,1024]{1,0:T(8,128)(2,1)} %gate.7), custom_call_target="tpu_custom_call" | custom-call | flops 32505856000 | tf_op jit(solution)/shard_map/pallas_call | solution.py:29
  1.7 1.6 %collective-permute-start = (bf16[16,1024]{1,0:T(8,128)(2,1)S(1)}, bf16[16,1024]{1,0:T(8,128)(2,1)S(1)}, u32[]{:S(2)}, u32[]{:S(2)}) collective-permute-start(bf16[16,1024]{1,0:T(8,128)(2,1)S(1)} %get-tuple-element.38), channel_id=1, source_target_pairs={{0,2},{4,6},{8,10},{12,14},{16,18},{20,22},{24,26},{28,30},{2,0},{... | collective-permute-start | bytes 98312 | tf_op jit(solution)/shard_map/ppermute | solution.py:481
  3.3 3.4 %collective-permute-start.1 = (bf16[16,1024]{1,0:T(8,128)(2,1)S(1)}, bf16[16,1024]{1,0:T(8,128)(2,1)S(1)}, u32[]{:S(2)}, u32[]{:S(2)}) collective-permute-start(bf16[16,1024]{1,0:T(8,128)(2,1)S(1)} %get-tuple-element.39), channel_id=1, source_target_pairs={{2,4},{6,8},{10,12},{14,16},{18,20},{22,24},{26,28},{4,2},{8,6},{1... | collective-permute-start | bytes 98312 | tf_op jit(solution)/shard_map/ppermute | solution.py:480
  6.7 1.0 %shard_map.111 = (f32[8,288,128]{2,1,0:T(8,128)S(1)}, f32[4,256,128]{2,1,0:T(8,128)S(1)}) custom-call(bf16[256,1024]{1,0:T(8,128)(2,1)S(1)} %copy-done.1, bf16[256,1024]{1,0:T(8,128)(2,1)S(1)} %copy-done.2, bf16[256,2048]{1,0:T(8,128)(2,1)S(1)} %copy-done.3, bf16[1024,2048]{1,0:T(8,128)(2,1)S(1)} %copy-done), custom_call_target="tpu_custom_call" | custom-call | flops 32505856 | tf_op jit(solution)/shard_map/pallas_call | solution.py:29
  7.7 2.1 %shard_map.112 = (f32[8,256,128]{2,1,0:T(8,128)S(1)}, f32[2,256,128]{2,1,0:T(8,128)S(1)}) custom-call(f32[8,288,128]{2,1,0:T(8,128)S(1)} %get-tuple-element.40.gated.gated_in, f32[31,1024]{1,0:T(8,128)S(1)} %copy-done.4), custom_call_target="tpu_custom_call" | custom-call | flops 16252928 | tf_op jit(solution)/shard_map/pallas_call | solution.py:29
  9.9 0.0 collective-permute-done.from_even
  9.9 1.1 %collective-permute-done.1.from_odd = bf16[16,1024]{1,0:T(8,128)(2,1)S(1)} collective-permute-done((bf16[16,1024]{1,0:T(8,128)(2,1)S(1)}, bf16[16,1024]{1,0:T(8,128)(2,1)S(1)}, u32[]{:S(2)}, u32[]{:S(2)}) %collective-permute-start.1) | collective-permute-done | bytes 32800 | tf_op jit(solution)/shard_map/ppermute | solution.py:480
  11.0 0.7 %shard_map.113 = (f32[8,288,128]{2,1,0:T(8,128)S(1)}, f32[8,256,128]{2,1,0:T(8,128)S(1)}, f32[2,256,128]{2,1,0:T(8,128)S(1)}, f32[1,512]{1,0:T(1,128)S(1)}) custom-call(bf16[16,1024]{1,0:T(8,128)(2,1)S(1)} %collective-permute-done.from_even, ...), custom_call_target="tpu_custom_call", output_to_operand_aliasing={{0}: (3, {}), {1}: (4, {}), {2}: (5, {})} | custom-call | flops 16252928 | tf_op jit(solution)/shard_map/pallas_call | solution.py:29
  11.7 0.1 collective-permute-start.2
  11.7 0.7 %shard_map.114.mix_high = f32[4,256,128]{2,1,0:T(8,128)S(1)} custom-call(bf16[256,2048]{1,0:T(8,128)(2,1)S(1)} %copy-done.3, bf16[1024,2048]{1,0:T(8,128)(2,1)S(1)} %copy-done), custom_call_target="tpu_custom_call" | custom-call | flops 16252928 | tf_op jit(solution)/shard_map/pallas_call | solution.py:29
  12.5 0.4 collective-permute-done.2.stats_other
  12.9 0.8 %shard_map.116 = (f32[8,128,128]{2,1,0:T(8,128)S(1)}, f32[8,128,128]{2,1,0:T(8,128)S(1)}, f32[1,256]{1,0:T(1,128)S(1)}, f32[2,8,128]{2,1,0:T(8,128)S(1)}) custom-call(f32[8,256,128]{2,1,0:T(8,128)S(1)} %get-tuple-element.43.conv, f32[4,256,128]{2,1,0:T(8,128)S(1)} %get-tuple-element.44.mix_low, f32[4,256,128]{2,1,0:T(8,128)S(1)} %shard_map.114.mix_high, ...), custom_call_target="tpu_custom_call" | custom-call | flops 8126464 | tf_op jit(solution)/shard_map/pallas_call | solution.py:29
  13.7 0.2 collective-permute-start.4
  13.9 0.8 %shard_map.115 = (f32[8,128,128]{2,1,0:T(8,128)S(1)}, f32[8,128,128]{2,1,0:T(8,128)S(1)}, f32[1,256]{1,0:T(1,128)S(1)}, f32[2,8,128]{2,1,0:T(8,128)S(1)}) custom-call(f32[8,256,128]{2,1,0:T(8,128)S(1)} %get-tuple-element.43.conv, f32[4,256,128]{2,1,0:T(8,128)S(1)} %get-tuple-element.44.mix_low, f32[4,256,128]{2,1,0:T(8,128)S(1)} %shard_map.114.mix_high, ...), custom_call_target="tpu_custom_call" | custom-call | flops 8126464 | tf_op jit(solution)/shard_map/pallas_call | solution.py:29
  14.7 0.4 collective-permute-start.3
  15.1 0.0 collective-permute-done.4.second_other
  15.1 1.6 %shard_map.117 = (f32[8,288,128]{2,1,0:T(8,128)S(1)}, f32[272,128]{1,0:T(8,128)S(1)}) custom-call(f32[8,128,128]{2,1,0:T(8,128)S(1)} %get-tuple-element.52.normed, f32[8,128,128]{2,1,0:T(8,128)S(1)} %get-tuple-element.53.grad, f32[1,512]{1,0:T(1,128)S(1)} %get-tuple-element.45.stats, f32[1,512]{1,0:T(1,128)S(1)} %collective-permute-done.2.stats_other, ...), custom_call_target="tpu_custom_call" | custom-call | flops 8126464 | tf_op jit(solution)/shard_map/pallas_call | solution.py:29
  16.7 1.7 %shard_map.118 = (f32[8,288,128]{2,1,0:T(8,128)S(1)}, bf16[400,128]{1,0:T(8,128)(2,1)S(1)}, bf16[128,128]{1,0:T(8,128)(2,1)S(1)}) custom-call(f32[8,128,128]{2,1,0:T(8,128)S(1)} %get-tuple-element.46.normed, f32[8,128,128]{2,1,0:T(8,128)S(1)} %get-tuple-element.47.grad, f32[1,512]{1,0:T(1,128)S(1)} %get-tuple-element.45.stats, ...), custom_call_target="tpu_custom_call", output_to_operand_aliasing={{0}: (9, {})} | custom-call | flops 8126464 | tf_op jit(solution)/shard_map/pallas_call | solution.py:29
  18.4 0.6 %collective-permute-start.5 = (bf16[400,128]{1,0:T(8,128)(2,1)S(1)}, bf16[400,128]{1,0:T(8,128)(2,1)S(1)}, u32[]{:S(2)}, u32[]{:S(2)}) collective-permute-start(bf16[400,128]{1,0:T(8,128)(2,1)S(1)} %get-tuple-element.58.mine), channel_id=1, source_target_pairs={{0,2},{2,0},{4,6},{6,4},{8,10},{10,8},{12,14},{14,12},{16,18},{18,... | collective-permute-start | bytes 307208 | tf_op jit(solution)/shard_map/ppermute | solution.py:550
  19.0 4.2 %collective-permute-done.5.other.refs_0_ = bf16[400,128]{1,0:T(8,128)(2,1)S(1)} collective-permute-done((bf16[400,128]{1,0:T(8,128)(2,1)S(1)}, bf16[400,128]{1,0:T(8,128)(2,1)S(1)}, u32[]{:S(2)}, u32[]{:S(2)}) %collective-permute-start.5) | collective-permute-done | bytes 102432 | tf_op jit(solution)/shard_map/ppermute | solution.py:550
  23.1 0.7 %collective-permute-start.6 = (bf16[400,128]{1,0:T(8,128)(2,1)S(1)}, bf16[400,128]{1,0:T(8,128)(2,1)S(1)}, u32[]{:S(2)}, u32[]{:S(2)}) collective-permute-start(bf16[400,128]{1,0:T(8,128)(2,1)S(1)} %shard_map.119.mine), channel_id=1, source_target_pairs={{0,4},{2,6},{4,0},{6,2},{8,12},{10,14},{12,8},{14,10},{16,20},{18,... | collective-permute-start | bytes 307208 | tf_op jit(solution)/shard_map/ppermute | solution.py:550
  23.8 1.7 %shard_map.120 = (bf16[112,1024]{1,0:T(8,128)(2,1)S(1)}, bf16[112,1024]{1,0:T(8,128)(2,1)S(1)}) custom-call(f32[8,288,128]{2,1,0:T(8,128)S(1)} %get-tuple-element.57.grad_conv, f32[31,1024]{1,0:T(8,128)S(1)} %copy-done.4, bf16[256,1024]{1,0:T(8,128)(2,1)S(1)} %copy-done.1, bf16[256,1024]{1,0:T(8,128)(2,1)S(1)} %copy-done.2), custom_call_target="tpu_custom_call" | custom-call | flops 8126464 | tf_op jit(solution)/shard_map/pallas_call | solution.py:29
  25.5 2.4 %collective-permute-done.6.refs_1_.other = bf16[400,128]{1,0:T(8,128)(2,1)S(1)} collective-permute-done((bf16[400,128]{1,0:T(8,128)(2,1)S(1)}, bf16[400,128]{1,0:T(8,128)(2,1)S(1)}, u32[]{:S(2)}, u32[]{:S(2)}) %collective-permute-start.6) | collective-permute-done | bytes 102432 | tf_op jit(solution)/shard_map/ppermute | solution.py:550
  27.9 0.1 collective-permute-start.8
  28.0 1.7 %shard_map.121 = (bf16[112,1024]{1,0:T(8,128)(2,1)S(1)}, bf16[112,1024]{1,0:T(8,128)(2,1)S(1)}, bf16[256,1024]{1,0:T(8,128)(2,1)}, bf16[256,1024]{1,0:T(8,128)(2,1)}) custom-call(f32[8,288,128]{2,1,0:T(8,128)S(1)} %get-tuple-element.57.grad_conv, f32[31,1024]{1,0:T(8,128)S(1)} %copy-done.4, bf16[256,1024]{1,0:T(8,128)(2,1)S(1)} %copy-done.1, ...), custom_call_target="tpu_custom_call" | custom-call | flops 8126464 | tf_op jit(solution)/shard_map/pallas_call | solution.py:29
  29.7 2.6 %collective-permute-done.8.other = bf16[272,128]{1,0:T(8,128)(2,1)S(1)} collective-permute-done((bf16[272,128]{1,0:T(8,128)(2,1)S(1)}, bf16[272,128]{1,0:T(8,128)(2,1)S(1)}, u32[]{:S(2)}, u32[]{:S(2)}) %collective-permute-start.8) | collective-permute-done | bytes 69664 | tf_op jit(solution)/shard_map/ppermute | solution.py:550
  32.3 2.6 %collective-permute-start.9 = (bf16[272,128]{1,0:T(8,128)(2,1)S(1)}, bf16[272,128]{1,0:T(8,128)(2,1)S(1)}, u32[]{:S(2)}, u32[]{:S(2)}) collective-permute-start(bf16[272,128]{1,0:T(8,128)(2,1)S(1)} %shard_map.124.mine), channel_id=1, source_target_pairs={{0,16},{2,18},{4,20},{6,22},{8,24},{10,26},{12,28},{14,30},{16,0},... | collective-permute-start | bytes 208904 | tf_op jit(solution)/shard_map/ppermute | solution.py:550
  34.9 3.3 %collective-permute-start.7 = (bf16[128,128]{1,0:T(8,128)(2,1)S(1)}, bf16[128,128]{1,0:T(8,128)(2,1)S(1)}, u32[]{:S(2)}, u32[]{:S(2)}) collective-permute-start(bf16[128,128]{1,0:T(8,128)(2,1)S(1)} %get-tuple-element.59), channel_id=1, source_target_pairs={{2,4},{6,8},{10,12},{14,16},{18,20},{22,24},{26,28},{4,2},{8,6},{1... | collective-permute-start | bytes 98312 | tf_op jit(solution)/shard_map/ppermute | solution.py:558
  38.2 4.3 %collective-permute-done.7.refs_2_ = bf16[128,128]{1,0:T(8,128)(2,1)S(1)} collective-permute-done((bf16[128,128]{1,0:T(8,128)(2,1)S(1)}, bf16[128,128]{1,0:T(8,128)(2,1)S(1)}, u32[]{:S(2)}, u32[]{:S(2)}) %collective-permute-start.7) | collective-permute-done | bytes 32800 | tf_op jit(solution)/shard_map/ppermute | solution.py:558
  42.5 1.6 %shard_map.122 = (f32[8,288,128]{2,1,0:T(8,128)S(1)}, bf16[256,1024]{1,0:T(8,128)(2,1)}, bf16[256,1024]{1,0:T(8,128)(2,1)}) custom-call(f32[8,288,128]{2,1,0:T(8,128)S(1)} %get-tuple-element.57.grad_conv, f32[31,1024]{1,0:T(8,128)S(1)} %copy-done.4, bf16[256,1024]{1,0:T(8,128)(2,1)S(1)} %copy-done.1, ...), custom_call_target="tpu_custom_call", output_to_operand_aliasing={{0}: (0, {}), {1}: (9, {}), {2}: (10, {})} | custom-call | flops 2031616 | tf_op jit(solution)/shard_map/pallas_call | solution.py:29
  44.1 0.0 collective-permute-done.9.other
  44.1 0.7 %shard_map.125 = (f32[31,1024]{1,0:T(8,128)}, f32[8,128]{1,0:T(8,128)}, f32[8,128]{1,0:T(8,128)}) custom-call(bf16[272,128]{1,0:T(8,128)(2,1)S(1)} %shard_map.124.mine, bf16[272,128]{1,0:T(8,128)(2,1)S(1)} %collective-permute-done.9.other), custom_call_target="tpu_custom_call" | custom-call | tf_op jit(solution)/shard_map/pallas_call | solution.py:29
  (18 shorter events, 0.1 us)
Async XLA Ops:
  0.6 6.1 %copy-start.1 = (bf16[256,1024]{1,0:T(8,128)(2,1)S(1)}, bf16[256,1024]{1,0:T(8,128)(2,1)}, u32[]{:S(2)}) copy-start(bf16[256,1024]{1,0:T(8,128)(2,1)} %value.7) | copy-start | bytes 1572868
  0.6 6.1 %copy-start.2 = (bf16[256,1024]{1,0:T(8,128)(2,1)S(1)}, bf16[256,1024]{1,0:T(8,128)(2,1)}, u32[]{:S(2)}) copy-start(bf16[256,1024]{1,0:T(8,128)(2,1)} %gate.7) | copy-start | bytes 1572868
  0.7 6.1 %copy-start.3 = (bf16[256,2048]{1,0:T(8,128)(2,1)S(1)}, bf16[256,2048]{1,0:T(8,128)(2,1)}, u32[]{:S(2)}) copy-start(bf16[256,2048]{1,0:T(8,128)(2,1)} %grads.3) | copy-start | bytes 3145732
  0.7 6.1 %copy-start = (bf16[1024,2048]{1,0:T(8,128)(2,1)S(1)}, bf16[1024,2048]{1,0:T(8,128)(2,1)}, u32[]{:S(2)}) copy-start(bf16[1024,2048]{1,0:T(8,128)(2,1)} %w.3) | copy-start | bytes 12582916
  1.7 8.2 %collective-permute-start = (bf16[16,1024]{1,0:T(8,128)(2,1)S(1)}, bf16[16,1024]{1,0:T(8,128)(2,1)S(1)}, u32[]{:S(2)}, u32[]{:S(2)}) collective-permute-start(bf16[16,1024]{1,0:T(8,128)(2,1)S(1)} %get-tuple-element.38), channel_id=1, source_target_pairs={{0,2},{4,6},{8,10},{12,14},{16,18},{20,22},{24,26},{28,30},{2,0},{... | collective-permute-start | bytes 98312 | tf_op jit(solution)/shard_map/ppermute | solution.py:481
  3.3 4.5 %copy-start.4 = (f32[31,1024]{1,0:T(8,128)S(1)}, f32[31,1024]{1,0:T(8,128)}, u32[]{:S(2)}) copy-start(f32[31,1024]{1,0:T(8,128)} %taps.9) | copy-start | bytes 380932
  3.3 7.7 %collective-permute-start.1 = (bf16[16,1024]{1,0:T(8,128)(2,1)S(1)}, bf16[16,1024]{1,0:T(8,128)(2,1)S(1)}, u32[]{:S(2)}, u32[]{:S(2)}) collective-permute-start(bf16[16,1024]{1,0:T(8,128)(2,1)S(1)} %get-tuple-element.39), channel_id=1, source_target_pairs={{2,4},{6,8},{10,12},{14,16},{18,20},{22,24},{26,28},{4,2},{8,6},{1... | collective-permute-start | bytes 98312 | tf_op jit(solution)/shard_map/ppermute | solution.py:480
  11.7 1.2 %copy-start.5 = (f32[1024]{0:T(1024)S(1)}, f32[1024]{0:T(1024)}, u32[]{:S(2)}) copy-start(f32[1024]{0:T(1024)} %param.10) | copy-start | bytes 12292
  11.7 1.2 %copy-start.6 = (f32[1024]{0:T(1024)S(1)}, f32[1024]{0:T(1024)}, u32[]{:S(2)}) copy-start(f32[1024]{0:T(1024)} %param.11) | copy-start | bytes 12292
  11.7 1.2 %collective-permute-start.2 = (f32[1,512]{1,0:T(1,128)S(1)}, f32[1,512]{1,0:T(1,128)S(1)}, u32[]{:S(2)}, u32[]{:S(2)}) collective-permute-start(f32[1,512]{1,0:T(1,128)S(1)} %get-tuple-element.45.stats), channel_id=1, source_target_pairs={{0,1},{1,0},{2,3},{3,2},{4,5},{5,4},{6,7},{7,6},{8,9},{9,8},{10,11... | collective-permute-start | bytes 6152 | tf_op jit(solution)/shard_map/ppermute | solution.py:421
  13.7 1.4 %collective-permute-start.4 = (f32[1,256]{1,0:T(1,128)S(1)}, f32[1,256]{1,0:T(1,128)S(1)}, u32[]{:S(2)}, u32[]{:S(2)}) collective-permute-start(f32[1,256]{1,0:T(1,128)S(1)} %get-tuple-element.54.second), channel_id=1, source_target_pairs={{0,1},{1,0},{2,3},{3,2},{4,5},{5,4},{6,7},{7,6},{8,9},{9,8},{10,11... | collective-permute-start | bytes 3080 | tf_op jit(solution)/shard_map/ppermute | solution.py:421
  14.7 2.0 %collective-permute-start.3 = (f32[1,256]{1,0:T(1,128)S(1)}, f32[1,256]{1,0:T(1,128)S(1)}, u32[]{:S(2)}, u32[]{:S(2)}) collective-permute-start(f32[1,256]{1,0:T(1,128)S(1)} %get-tuple-element.48.second), channel_id=1, source_target_pairs={{0,1},{1,0},{2,3},{3,2},{4,5},{5,4},{6,7},{7,6},{8,9},{9,8},{10,11... | collective-permute-start | bytes 3080 | tf_op jit(solution)/shard_map/ppermute | solution.py:421
  18.4 4.7 %collective-permute-start.5 = (bf16[400,128]{1,0:T(8,128)(2,1)S(1)}, bf16[400,128]{1,0:T(8,128)(2,1)S(1)}, u32[]{:S(2)}, u32[]{:S(2)}) collective-permute-start(bf16[400,128]{1,0:T(8,128)(2,1)S(1)} %get-tuple-element.58.mine), channel_id=1, source_target_pairs={{0,2},{2,0},{4,6},{6,4},{8,10},{10,8},{12,14},{14,12},{16,18},{18,... | collective-permute-start | bytes 307208 | tf_op jit(solution)/shard_map/ppermute | solution.py:550
  23.1 4.7 %collective-permute-start.6 = (bf16[400,128]{1,0:T(8,128)(2,1)S(1)}, bf16[400,128]{1,0:T(8,128)(2,1)S(1)}, u32[]{:S(2)}, u32[]{:S(2)}) collective-permute-start(bf16[400,128]{1,0:T(8,128)(2,1)S(1)} %shard_map.119.mine), channel_id=1, source_target_pairs={{0,4},{2,6},{4,0},{6,2},{8,12},{10,14},{12,8},{14,10},{16,20},{18,... | collective-permute-start | bytes 307208 | tf_op jit(solution)/shard_map/ppermute | solution.py:550
  27.9 4.4 %collective-permute-start.8 = (bf16[272,128]{1,0:T(8,128)(2,1)S(1)}, bf16[272,128]{1,0:T(8,128)(2,1)S(1)}, u32[]{:S(2)}, u32[]{:S(2)}) collective-permute-start(bf16[272,128]{1,0:T(8,128)(2,1)S(1)} %shard_map.123.mine), channel_id=1, source_target_pairs={{0,8},{2,10},{4,12},{6,14},{8,0},{10,2},{12,4},{14,6},{16,24},{18,... | collective-permute-start | bytes 208904 | tf_op jit(solution)/shard_map/ppermute | solution.py:550
  32.3 11.8 %collective-permute-start.9 = (bf16[272,128]{1,0:T(8,128)(2,1)S(1)}, bf16[272,128]{1,0:T(8,128)(2,1)S(1)}, u32[]{:S(2)}, u32[]{:S(2)}) collective-permute-start(bf16[272,128]{1,0:T(8,128)(2,1)S(1)} %shard_map.124.mine), channel_id=1, source_target_pairs={{0,16},{2,18},{4,20},{6,22},{8,24},{10,26},{12,28},{14,30},{16,0},... | collective-permute-start | bytes 208904 | tf_op jit(solution)/shard_map/ppermute | solution.py:550
  34.9 7.6 %collective-permute-start.7 = (bf16[128,128]{1,0:T(8,128)(2,1)S(1)}, bf16[128,128]{1,0:T(8,128)(2,1)S(1)}, u32[]{:S(2)}, u32[]{:S(2)}) collective-permute-start(bf16[128,128]{1,0:T(8,128)(2,1)S(1)} %get-tuple-element.59), channel_id=1, source_target_pairs={{2,4},{6,8},{10,12},{14,16},{18,20},{22,24},{26,28},{4,2},{8,6},{1... | collective-permute-start | bytes 98312 | tf_op jit(solution)/shard_map/ppermute | solution.py:558
where the time goes:
time: 44.9 us; the launch traced here: 44.8 us
  Pallas kernels  16 us (36%)
  waiting for transfers between devices  15 us (33%)
  starting transfers between devices  12.9 us (29%)
  between operations  0.85 us (2%)
    pallas_call x16, Pallas kernels, call(): pl.pallas_call(body, out_shape=[jax.ShapeDtypeStruct(shape, dtype) for sh...  16 us
    ppermute x4, waiting for transfers between devices, exchange(): return lax.ppermute(array, ('sp', 'tp'), pairs)  9.14 us
    ppermute x1, waiting for transfers between devices, shards(): grads_odd = lax.ppermute(send_odd, 'sp', swap_odd)  4.31 us
    ppermute x4, starting transfers between devices, exchange(): return lax.ppermute(array, ('sp', 'tp'), pairs)  3.96 us
    ppermute x1, starting transfers between devices, shards(): from_odd = lax.ppermute(send_odd, 'sp', swap_odd)  3.4 us
    ppermute x1, starting transfers between devices, shards(): grads_odd = lax.ppermute(send_odd, 'sp', swap_odd)  3.27 us
    ppermute x1, starting transfers between devices, shards(): from_even = lax.ppermute(send_even, 'sp', swap_even)  1.56 us
    ppermute x1, waiting for transfers between devices, shards(): from_odd = lax.ppermute(send_odd, 'sp', swap_odd)  1.12 us
  transfers between devices with their start and end apart: 10, of which 6 were waited for; matrix products, arithmetic and copies ran while one was open for 0% of the time, Pallas kernels for 25%

commit v1 on v0

--- a/solution.py
+++ b/solution.py
@@ -122,14 +122,28 @@
     lax.fori_loop(0, (last - first) // 16, sums, 0)
 
 
-def conv_inner(pad, gated, taps, out, part):
+def conv_inner(pad, gated, taps, out, part, middle, low_gap, high_gap):
     blocks, height, _ = out.shape
-    shift = pad - taps.shape[0] // 2
+    kernel = taps.shape[0]
+    shift = pad - kernel // 2
+    rows = height - 2 * pad
 
     def body(block, carry):
         lanes = pl.ds(pl.multiple_of(block * LANES, LANES), LANES)
-        for at, count in pieces(pad, height - pad, 56):
-            out[block, at : at + count, :] = conv_rows(taps, gated, block, lanes, at, count, shift)
+        split_rows(gated, block, pad + shift, rows // 2 + kernel // 2, middle, low_gap, high_gap)
+        for at, count in pieces(0, rows // 2, 56):
+            both, even, odd = (jnp.zeros((count, LANES), F32) for _ in range(3))
+            for pair in range(kernel // 2 + 1):
+                span = pl.ds(at + pair, count)
+                first = taps[pl.ds(2 * pair, 1), lanes]
+                even = even + first * low_gap[span, :]
+                if 2 * pair + 1 < kernel:
+                    second = taps[pl.ds(2 * pair + 1, 1), lanes]
+                    odd = odd + second * high_gap[span, :]
+                    first = first + second
+                both = both + first * middle[span, :]
+            out[block, pl.ds(pad + 2 * at, count, stride=2), :] = both + even
+            out[block, pl.ds(pad + 2 * at + 1, count, stride=2), :] = both + odd
         return carry
 
     lax.fori_loop(0, blocks, body, 0)
@@ -152,27 +166,18 @@
 
 
 def lane_sums(first, second):
-    stacked = jnp.concatenate([first[...], second[...]], 0)
-    split = jnp.concatenate(thirds(stacked), 1).astype(BF16)
-    ones = jnp.ones((16, split.shape[1]), BF16)
-    return lax.dot_general(
-        ones, split, (((1,), (1,)), ((), ())), preferred_element_type=F32
-    )[0:1]
-
-
-def spread(lines):
-    rows = [row for line in lines for row in thirds(line)]
-    rows += [jnp.zeros_like(lines[0])] * (16 - len(rows))
-    shape = (16, len(lines) * LANES)
-    part = lax.broadcasted_iota(jnp.int32, shape, 0)
-    block = lax.broadcasted_iota(jnp.int32, shape, 1) // LANES
-    chosen = jnp.logical_and(part >= 3 * block, part < 3 * block + 3)
-    return lax.dot_general(
-        jnp.concatenate(rows, 0).astype(BF16),
-        chosen.astype(F32).astype(BF16),
-        (((0,), (0,)), ((), ())),
-        preferred_element_type=F32,
-    )
+    split = jnp.concatenate([*thirds(first[...]), *thirds(second[...])], 1).astype(BF16)
+    shape = (split.shape[1], LANES)
+    late = lax.broadcasted_iota(jnp.int32, shape, 0) >= 3 * LANES
+    right = lax.broadcasted_iota(jnp.int32, shape, 1) >= LANES // 2
+    chosen = jnp.where(late == right, 1.0, 0.0).astype(BF16)
+    return jnp.dot(split, chosen, preferred_element_type=F32)
+
+
+def spread(pair):
+    left = lax.broadcasted_iota(jnp.int32, pair.shape, 1) < LANES // 2
+    turned = pltpu.roll(pair, LANES // 2, 1)
+    return jnp.where(left, pair, turned), jnp.where(left, turned, pair)
 
 
 def conv_edges(pad, from_even, from_odd, taps, gated_in, conv_in, part_in, gated, conv, part, stats):
@@ -192,12 +197,9 @@
     stats[...] = lane_sums(part[0], part[1])
 
 
-def moments(mine, other, width):
-    total = (mine[...] + other[...]) / width
-    rows = total.shape[1] // 2
-    mean = total[:, :rows]
-    var = total[:, rows:] - mean * mean
-    return mean, lax.rsqrt(var + EPS)
+def moments(mine, other, width, rows):
+    mean, square = spread((mine[rows, :] + other[rows, :]) / width)
+    return mean, lax.rsqrt(square - mean * mean + EPS)
 
 
 def norm_back(
@@ -219,8 +221,9 @@
 ):
     blocks, height, _ = normed.shape
     half = mix_low.shape[0]
-    mean, inv = moments(stats, stats_other, width)
-    line[...] = spread([mean[:, at : at + height], inv[:, at : at + height]])
+    mean, inv = moments(stats, stats_other, width, slice(at, at + height))
+    line[:, :LANES] = mean
+    line[:, LANES:] = inv
 
     def body(chunk, carry):
         rows = pl.ds(pl.multiple_of(chunk * 16, 16), 16)
@@ -257,6 +260,19 @@
     second[...] = lane_sums(part[0], part[1])
 
 
+def split_rows(source, block, at, count, middle, low_gap, high_gap):
+    even = source[block, pl.ds(at, count, stride=2), :]
+    odd = source[block, pl.ds(at + 1, count, stride=2), :]
+    after = source[block, pl.ds(at + 2, count, stride=2), :]
+    middle[:count, :] = odd
+    low_gap[:count, :] = even - odd
+    high_gap[:count, :] = after - odd
+
+
+def fold(term):
+    return (term[0:8] + term[8:16]) + (term[16:24] + term[24:32])
+
+
 def tap_sums(
     pad, width, kernel, at, height, normed, grad, stats, stats_other, second, second_other, gated, *refs
 ):
@@ -266,14 +282,14 @@
     odd = parity() == 1
     final = at + count == height
     if final:
-        sums_low, sums_high, _, raw_in, grad_conv, packed, send_odd, line, raw = refs
+        sums_low, sums_high, _, raw_in, grad_conv, packed, send_odd, line, *split, raw = refs
     else:
-        grad_conv, raw, line = refs
-    _, inv = moments(stats, stats_other, width)
-    total = (second[...] + second_other[...]) / width
-    line[...] = spread([inv[:, at : at + count], total[:, :count], total[:, count:]])
-    if not final:
-        raw[...] = jnp.zeros_like(raw)
+        grad_conv, raw, line, *split = refs
+    middle, low_gap, high_gap = split
+    line[:, :LANES] = moments(stats, stats_other, width, slice(at, at + count))[1]
+    means = spread((second[...] + second_other[...]) / width)
+    line[:, LANES : 2 * LANES] = means[0]
+    line[:, 2 * LANES :] = means[1]
 
     def body(block, carry):
         for low, size in pieces(0, count, 32):
@@ -284,21 +300,30 @@
                 - normed[block, span, :] * line[span, 2 * LANES :]
             )
         base = pl.multiple_of(block * each, each)
-        for low in range(0, kernel, 16):
-            taps = range(low, min(low + 16, kernel))
-            totals = [jnp.zeros((8, LANES), F32) for _ in taps]
-            for row in range(at, at + count, 32):
-                own = grad_conv[block, pad + row : pad + row + 32, :]
-                for index, tap in enumerate(taps):
-                    term = own * gated[block, pl.ds(row + tap + shift, 32), :]
-                    totals[index] = totals[index] + (
-                        (term[0:8] + term[8:16]) + (term[16:24] + term[24:32])
-                    )
-            for index, tap in enumerate(taps):
-                line_sum = jnp.sum(totals[index], 0, keepdims=True)
-                if final:
-                    line_sum += raw_in[pl.ds(base + tap, 1), :]
-                raw[pl.ds(base + tap, 1), :] = line_sum
+        split_rows(gated, block, at + shift, count // 2 + kernel // 2, middle, low_gap, high_gap)
+        for low in range(0, kernel // 2 + 1, 8):
+            pairs = range(low, min(low + 8, kernel // 2 + 1))
+            both, evens, odds = ([jnp.zeros((8, LANES), F32) for _ in pairs] for _ in range(3))
+            for row in range(0, count // 2, 32):
+                even = grad_conv[block, pl.ds(pad + at + 2 * row, 32, stride=2), :]
+                odd_rows = grad_conv[block, pl.ds(pad + at + 2 * row + 1, 32, stride=2), :]
+                together = even + odd_rows
+                for index, pair in enumerate(pairs):
+                    span = pl.ds(row + pair, 32)
+                    both[index] = both[index] + fold(together * middle[span, :])
+                    evens[index] = evens[index] + fold(even * low_gap[span, :])
+                    if 2 * pair + 1 < kernel:
+                        odds[index] = odds[index] + fold(odd_rows * high_gap[span, :])
+            for index, pair in enumerate(pairs):
+                for tap, total in ((2 * pair, evens[index]), (2 * pair + 1, odds[index])):
+                    if tap < kernel:
+                        total = both[index] + total
+                        tile = pl.ds(pl.multiple_of((base + tap) * 8, 8), 8)
+                        if final:
+                            total = jnp.sum(total + raw_in[tile, :], 0, keepdims=True)
+                            raw[pl.ds(base + tap, 1), :] = total
+                        else:
+                            raw[tile, :] = total
         if final:
             one = pl.ds(block, 1)
             raw[pl.ds(base + kernel, 1), :] = sums_low[0, one, :] + sums_high[0, one, :]
@@ -310,7 +335,7 @@
         return carry
 
     if final:
-        raw[blocks * each :, :] = raw_in[blocks * each :, :]
+        raw[blocks * each :, :] = jnp.zeros((raw.shape[0] - blocks * each, LANES), F32)
     lax.fori_loop(0, blocks, body, 0)
     if final:
         raw[blocks * each : blocks * each + blocks, :] = sums_low[1] + sums_high[1]
@@ -457,7 +482,7 @@
     each = up(kernel + 1, 16)
     wide = ((blocks, rows + 2 * pad, LANES), F32)
     frame = ((blocks, rows, LANES), F32)
-    lines = ((1, 2 * rows), F32)
+    lines = ((rows, LANES), F32)
     send = ((pad, channels), BF16)
     conv_flops = 2 * kernel * rows * channels
     swap_odd = [(i, i + 1) for i in range(1, count - 1, 2)]
@@ -479,7 +504,7 @@
     )
     from_odd = lax.ppermute(send_odd, "sp", swap_odd)
     from_even = lax.ppermute(send_even, "sp", swap_even)
-    low_blocks = channels // tile // 2 * tile // LANES
+    low_blocks = max(channels // tile // 4, 1) * tile // LANES
     high_blocks = blocks - low_blocks
     gated, mix_low = call(
         functools.partial(gate_and_mix, pad, tile),
@@ -491,6 +516,7 @@
         functools.partial(conv_inner, pad),
         [frame, ((2, rows, LANES), F32)],
         (gated, taps),
+        scratch=[pltpu.VMEM((up(rows // 2 + kernel // 2, 8), LANES), F32)] * 3,
         flops=conv_flops,
     )
     gated, conv, part, stats = call(
@@ -511,12 +537,13 @@
     packed_rows = up(blocks * each + blocks, 16)
     height = up(rows // 2, LANES) if rows > LANES else rows
     halves = [(at, min(height, rows - at)) for at in range(0, rows, height)]
-    assert len(halves) == 2
+    assert len(halves) == 2 and height % 64 == 0
+    gap = pltpu.VMEM((up(rows // 2 + kernel // 2, 8), LANES), F32)
     ready = []
     for at, size in halves:
         normed, grad, second, sums = call(
             functools.partial(norm_back, width, at),
-            [((blocks, size, LANES), F32)] * 2 + [((1, 2 * size), F32), ((2, blocks, LANES), F32)],
+            [((blocks, size, LANES), F32)] * 2 + [((size, LANES), F32), ((2, blocks, LANES), F32)],
             (conv, mix_low, mix_high, stats, stats_other, gain[None], shift[None]),
             scratch=[pltpu.VMEM((2, size, LANES), F32), pltpu.VMEM((size, 2 * LANES), F32)],
             flops=conv_flops // 2,
@@ -525,9 +552,9 @@
     (at, size), (next_at, next_size) = halves
     grad_conv, raw = call(
         functools.partial(tap_sums, pad, width, kernel, at, rows),
-        [wide, ((packed_rows, LANES), F32)],
+        [wide, ((blocks * each * 8, LANES), F32)],
         ready[0][:-1],
-        scratch=[pltpu.VMEM((size, 3 * LANES), F32)],
+        scratch=[pltpu.VMEM((size, 3 * LANES), F32)] + [gap] * 3,
         flops=conv_flops // 2,
     )
     grad_conv, packed, send_odd = call(
@@ -535,7 +562,7 @@
         [wide, ((packed_rows + blocks * pad, LANES), BF16), ((blocks * pad, LANES), BF16)],
         (*ready[1][:-1], ready[0][-1], ready[1][-1], grad_conv, raw),
         aliases={9: 0},
-        scratch=[pltpu.VMEM((next_size, 3 * LANES), F32), pltpu.VMEM((packed_rows, LANES), F32)],
+        scratch=[pltpu.VMEM((next_size, 3 * LANES), F32)] + [gap] * 3 + [pltpu.VMEM((packed_rows, LANES), F32)],
         flops=conv_flops // 2,
     )
     twos, odds = radices(count)

time: 44.9 us -> 44.4 us (0.989)
  Pallas kernels: 16 us -> 14.9 us
  waiting for transfers between devices: 15 us -> 16 us
  starting transfers between devices: 12.9 us -> 12.4 us
    pallas_call x16, Pallas kernels: 16 us -> 14.9 us  [call(): pl.pallas_call(body, out_shape=[jax.ShapeDtypeStruct(shape, dtype) for sh...]
    ppermute x1, waiting for transfers between devices: 1.12 us -> 1.69 us  [shards(): from_odd = lax.ppermute(send_odd, 'sp', swap_odd)]
    ppermute x4, waiting for transfers between devices: 9.14 us -> 9.62 us  [exchange(): return lax.ppermute(array, ('sp', 'tp'), pairs)]
    ppermute x4, starting transfers between devices: 3.96 us -> 3.48 us  [exchange(): return lax.ppermute(array, ('sp', 'tp'), pairs)]
  transfers between devices with their start and end apart: 10 -> 10, of which waited for: 6 -> 6; matrix products, arithmetic and copies ran while one was open for 0% -> 0% of each run, Pallas kernels for 25% -> 23%
where the time goes in v1:
time: 44.4 us; the launch traced here: 44.2 us
  waiting for transfers between devices  16 us (36%)
  Pallas kernels  14.9 us (34%)
  starting transfers between devices  12.4 us (28%)
  between operations  0.89 us (2%)
    pallas_call x16, Pallas kernels, call(): pl.pallas_call(body, out_shape=[jax.ShapeDtypeStruct(shape, dtype) for sh...  14.9 us
    ppermute x4, waiting for transfers between devices, exchange(): return lax.ppermute(array, ('sp', 'tp'), pairs)  9.62 us
    ppermute x1, waiting for transfers between devices, shards(): grads_odd = lax.ppermute(send_odd, 'sp', swap_odd)  4.31 us
    ppermute x4, starting transfers between devices, exchange(): return lax.ppermute(array, ('sp', 'tp'), pairs)  3.48 us
    ppermute x1, starting transfers between devices, shards(): from_odd = lax.ppermute(send_odd, 'sp', swap_odd)  3.4 us
    ppermute x1, starting transfers between devices, shards(): grads_odd = lax.ppermute(send_odd, 'sp', swap_odd)  3.27 us
    ppermute x1, waiting for transfers between devices, shards(): from_odd = lax.ppermute(send_odd, 'sp', swap_odd)  1.69 us
    ppermute x1, starting transfers between devices, shards(): from_even = lax.ppermute(send_even, 'sp', swap_even)  1.56 us
  transfers between devices with their start and end apart: 10, of which 6 were waited for; matrix products, arithmetic and copies ran while one was open for 0% of the time, Pallas kernels for 23%

profile of v1, /device:TPU:8, one launch (start us, length us, event | category | flops | bytes accessed | tf_op | source)
XLA Modules:
  0.0 44.2 jit_solution(16000609287011737614)
XLA Ops:
  0.7 1.0 %shard_map.110 = (bf16[16,1024]{1,0:T(8,128)(2,1)S(1)}, bf16[16,1024]{1,0:T(8,128)(2,1)S(1)}) custom-call(bf16[256,1024]{1,0:T(8,128)(2,1)} %value.7, bf16[256,1024]{1,0:T(8,128)(2,1)} %gate.7), custom_call_target="tpu_custom_call" | custom-call | flops 32505856000 | tf_op jit(solution)/shard_map/pallas_call | solution.py:29
  1.7 1.6 %collective-permute-start = (bf16[16,1024]{1,0:T(8,128)(2,1)S(1)}, bf16[16,1024]{1,0:T(8,128)(2,1)S(1)}, u32[]{:S(2)}, u32[]{:S(2)}) collective-permute-start(bf16[16,1024]{1,0:T(8,128)(2,1)S(1)} %get-tuple-element.38), channel_id=1, source_target_pairs={{0,2},{4,6},{8,10},{12,14},{16,18},{20,22},{24,26},{28,30},{2,0},{... | collective-permute-start | bytes 98312 | tf_op jit(solution)/shard_map/ppermute | solution.py:506
  3.3 3.4 %collective-permute-start.1 = (bf16[16,1024]{1,0:T(8,128)(2,1)S(1)}, bf16[16,1024]{1,0:T(8,128)(2,1)S(1)}, u32[]{:S(2)}, u32[]{:S(2)}) collective-permute-start(bf16[16,1024]{1,0:T(8,128)(2,1)S(1)} %get-tuple-element.39), channel_id=1, source_target_pairs={{2,4},{6,8},{10,12},{14,16},{18,20},{22,24},{26,28},{4,2},{8,6},{1... | collective-permute-start | bytes 98312 | tf_op jit(solution)/shard_map/ppermute | solution.py:505
  6.7 0.7 %shard_map.111 = (f32[8,288,128]{2,1,0:T(8,128)S(1)}, f32[2,256,128]{2,1,0:T(8,128)S(1)}) custom-call(bf16[256,1024]{1,0:T(8,128)(2,1)S(1)} %copy-done.1, bf16[256,1024]{1,0:T(8,128)(2,1)S(1)} %copy-done.2, bf16[256,2048]{1,0:T(8,128)(2,1)S(1)} %copy-done.3, bf16[1024,2048]{1,0:T(8,128)(2,1)S(1)} %copy-done), custom_call_target="tpu_custom_call" | custom-call | flops 32505856 | tf_op jit(solution)/shard_map/pallas_call | solution.py:29
  7.5 1.8 %shard_map.112 = (f32[8,256,128]{2,1,0:T(8,128)S(1)}, f32[2,256,128]{2,1,0:T(8,128)S(1)}) custom-call(f32[8,288,128]{2,1,0:T(8,128)S(1)} %get-tuple-element.40.gated.gated_in, f32[31,1024]{1,0:T(8,128)S(1)} %copy-done.4), custom_call_target="tpu_custom_call" | custom-call | flops 16252928 | tf_op jit(solution)/shard_map/pallas_call | solution.py:29
  9.3 1.7 %collective-permute-done.1.from_odd = bf16[16,1024]{1,0:T(8,128)(2,1)S(1)} collective-permute-done((bf16[16,1024]{1,0:T(8,128)(2,1)S(1)}, bf16[16,1024]{1,0:T(8,128)(2,1)S(1)}, u32[]{:S(2)}, u32[]{:S(2)}) %collective-permute-start.1) | collective-permute-done | bytes 32800 | tf_op jit(solution)/shard_map/ppermute | solution.py:505
  11.0 0.7 %shard_map.113 = (f32[8,288,128]{2,1,0:T(8,128)S(1)}, f32[8,256,128]{2,1,0:T(8,128)S(1)}, f32[2,256,128]{2,1,0:T(8,128)S(1)}, f32[256,128]{1,0:T(8,128)S(1)}) custom-call(bf16[16,1024]{1,0:T(8,128)(2,1)S(1)} %collective-permute-done.from_even, ...), custom_call_target="tpu_custom_call", output_to_operand_aliasing={{0}: (3, {}), {1}: (4, {}), {2}: (5, {})} | custom-call | flops 16252928 | tf_op jit(solution)/shard_map/pallas_call | solution.py:29
  11.7 0.0 copy-start.5
  11.7 0.0 copy-start.6
  11.7 0.1 collective-permute-start.2
  11.8 1.0 %shard_map.114.mix_high = f32[6,256,128]{2,1,0:T(8,128)S(1)} custom-call(bf16[256,2048]{1,0:T(8,128)(2,1)S(1)} %copy-done.3, bf16[1024,2048]{1,0:T(8,128)(2,1)S(1)} %copy-done), custom_call_target="tpu_custom_call" | custom-call | flops 16252928 | tf_op jit(solution)/shard_map/pallas_call | solution.py:29
  12.8 0.3 collective-permute-done.2.stats_other
  13.1 0.7 %shard_map.116 = (f32[8,128,128]{2,1,0:T(8,128)S(1)}, f32[8,128,128]{2,1,0:T(8,128)S(1)}, f32[128,128]{1,0:T(8,128)S(1)}, f32[2,8,128]{2,1,0:T(8,128)S(1)}) custom-call(f32[8,256,128]{2,1,0:T(8,128)S(1)} %get-tuple-element.43.conv, f32[2,256,128]{2,1,0:T(8,128)S(1)} %get-tuple-element.44.mix_low, f32[6,256,128]{2,1,0:T(8,128)S(1)} %shard_map.114.mix_high, ...), custom_call_target="tpu_custom_call" | custom-call | flops 8126464 | tf_op jit(solution)/shard_map/pallas_call | solution.py:29
  13.9 0.3 collective-permute-start.4
  14.1 0.7 %shard_map.115 = (f32[8,128,128]{2,1,0:T(8,128)S(1)}, f32[8,128,128]{2,1,0:T(8,128)S(1)}, f32[128,128]{1,0:T(8,128)S(1)}, f32[2,8,128]{2,1,0:T(8,128)S(1)}) custom-call(f32[8,256,128]{2,1,0:T(8,128)S(1)} %get-tuple-element.43.conv, f32[2,256,128]{2,1,0:T(8,128)S(1)} %get-tuple-element.44.mix_low, f32[6,256,128]{2,1,0:T(8,128)S(1)} %shard_map.114.mix_high, ...), custom_call_target="tpu_custom_call" | custom-call | flops 8126464 | tf_op jit(solution)/shard_map/pallas_call | solution.py:29
  14.8 0.4 collective-permute-start.3
  15.2 0.0 collective-permute-done.4.second_other
  15.2 1.2 %shard_map.117 = (f32[8,288,128]{2,1,0:T(8,128)S(1)}, f32[2048,128]{1,0:T(8,128)S(1)}) custom-call(f32[8,128,128]{2,1,0:T(8,128)S(1)} %get-tuple-element.52.normed, f32[8,128,128]{2,1,0:T(8,128)S(1)} %get-tuple-element.53.grad, f32[256,128]{1,0:T(8,128)S(1)} %get-tuple-element.45.stats, f32[256,128]{1,0:T(8,128)S(1)} %collective-permute-done.2.stats_other, ...), custom_call_target="tpu_custom_call" | custom-call | flops 8126464 | tf_op jit(solution)/shard_map/pallas_call | solution.py:29
  16.4 1.4 %shard_map.118 = (f32[8,288,128]{2,1,0:T(8,128)S(1)}, bf16[400,128]{1,0:T(8,128)(2,1)S(1)}, bf16[128,128]{1,0:T(8,128)(2,1)S(1)}) custom-call(f32[8,128,128]{2,1,0:T(8,128)S(1)} %get-tuple-element.46.normed, f32[8,128,128]{2,1,0:T(8,128)S(1)} %get-tuple-element.47.grad, f32[256,128]{1,0:T(8,128)S(1)} %get-tuple-element.45.stats, ...), custom_call_target="tpu_custom_call", output_to_operand_aliasing={{0}: (9, {})} | custom-call | flops 8126464 | tf_op jit(solution)/shard_map/pallas_call | solution.py:29
  17.9 0.1 collective-permute-start.5
  17.9 4.6 %collective-permute-done.5.other.refs_0_ = bf16[400,128]{1,0:T(8,128)(2,1)S(1)} collective-permute-done((bf16[400,128]{1,0:T(8,128)(2,1)S(1)}, bf16[400,128]{1,0:T(8,128)(2,1)S(1)}, u32[]{:S(2)}, u32[]{:S(2)}) %collective-permute-start.5) | collective-permute-done | bytes 102432 | tf_op jit(solution)/shard_map/ppermute | solution.py:577
  22.6 0.7 %collective-permute-start.6 = (bf16[400,128]{1,0:T(8,128)(2,1)S(1)}, bf16[400,128]{1,0:T(8,128)(2,1)S(1)}, u32[]{:S(2)}, u32[]{:S(2)}) collective-permute-start(bf16[400,128]{1,0:T(8,128)(2,1)S(1)} %shard_map.119.mine), channel_id=1, source_target_pairs={{0,4},{2,6},{4,0},{6,2},{8,12},{10,14},{12,8},{14,10},{16,20},{18,... | collective-permute-start | bytes 307208 | tf_op jit(solution)/shard_map/ppermute | solution.py:577
  23.3 1.6 %shard_map.120 = (bf16[112,1024]{1,0:T(8,128)(2,1)S(1)}, bf16[112,1024]{1,0:T(8,128)(2,1)S(1)}) custom-call(f32[8,288,128]{2,1,0:T(8,128)S(1)} %get-tuple-element.57.grad_conv, f32[31,1024]{1,0:T(8,128)S(1)} %copy-done.4, bf16[256,1024]{1,0:T(8,128)(2,1)S(1)} %copy-done.1, bf16[256,1024]{1,0:T(8,128)(2,1)S(1)} %copy-done.2), custom_call_target="tpu_custom_call" | custom-call | flops 8126464 | tf_op jit(solution)/shard_map/pallas_call | solution.py:29
  24.9 2.4 %collective-permute-done.6.refs_1_.other = bf16[400,128]{1,0:T(8,128)(2,1)S(1)} collective-permute-done((bf16[400,128]{1,0:T(8,128)(2,1)S(1)}, bf16[400,128]{1,0:T(8,128)(2,1)S(1)}, u32[]{:S(2)}, u32[]{:S(2)}) %collective-permute-start.6) | collective-permute-done | bytes 102432 | tf_op jit(solution)/shard_map/ppermute | solution.py:577
  27.4 0.1 collective-permute-start.8
  27.4 1.7 %shard_map.121 = (bf16[112,1024]{1,0:T(8,128)(2,1)S(1)}, bf16[112,1024]{1,0:T(8,128)(2,1)S(1)}, bf16[256,1024]{1,0:T(8,128)(2,1)}, bf16[256,1024]{1,0:T(8,128)(2,1)}) custom-call(f32[8,288,128]{2,1,0:T(8,128)S(1)} %get-tuple-element.57.grad_conv, f32[31,1024]{1,0:T(8,128)S(1)} %copy-done.4, bf16[256,1024]{1,0:T(8,128)(2,1)S(1)} %copy-done.1, ...), custom_call_target="tpu_custom_call" | custom-call | flops 8126464 | tf_op jit(solution)/shard_map/pallas_call | solution.py:29
  29.1 2.6 %collective-permute-done.8.other = bf16[272,128]{1,0:T(8,128)(2,1)S(1)} collective-permute-done((bf16[272,128]{1,0:T(8,128)(2,1)S(1)}, bf16[272,128]{1,0:T(8,128)(2,1)S(1)}, u32[]{:S(2)}, u32[]{:S(2)}) %collective-permute-start.8) | collective-permute-done | bytes 69664 | tf_op jit(solution)/shard_map/ppermute | solution.py:577
  31.7 2.6 %collective-permute-start.9 = (bf16[272,128]{1,0:T(8,128)(2,1)S(1)}, bf16[272,128]{1,0:T(8,128)(2,1)S(1)}, u32[]{:S(2)}, u32[]{:S(2)}) collective-permute-start(bf16[272,128]{1,0:T(8,128)(2,1)S(1)} %shard_map.124.mine), channel_id=1, source_target_pairs={{0,16},{2,18},{4,20},{6,22},{8,24},{10,26},{12,28},{14,30},{16,0},... | collective-permute-start | bytes 208904 | tf_op jit(solution)/shard_map/ppermute | solution.py:577
  34.4 3.3 %collective-permute-start.7 = (bf16[128,128]{1,0:T(8,128)(2,1)S(1)}, bf16[128,128]{1,0:T(8,128)(2,1)S(1)}, u32[]{:S(2)}, u32[]{:S(2)}) collective-permute-start(bf16[128,128]{1,0:T(8,128)(2,1)S(1)} %get-tuple-element.59), channel_id=1, source_target_pairs={{2,4},{6,8},{10,12},{14,16},{18,20},{22,24},{26,28},{4,2},{8,6},{1... | collective-permute-start | bytes 98312 | tf_op jit(solution)/shard_map/ppermute | solution.py:585
  37.7 4.3 %collective-permute-done.7.refs_2_ = bf16[128,128]{1,0:T(8,128)(2,1)S(1)} collective-permute-done((bf16[128,128]{1,0:T(8,128)(2,1)S(1)}, bf16[128,128]{1,0:T(8,128)(2,1)S(1)}, u32[]{:S(2)}, u32[]{:S(2)}) %collective-permute-start.7) | collective-permute-done | bytes 32800 | tf_op jit(solution)/shard_map/ppermute | solution.py:585
  42.0 1.6 %shard_map.122 = (f32[8,288,128]{2,1,0:T(8,128)S(1)}, bf16[256,1024]{1,0:T(8,128)(2,1)}, bf16[256,1024]{1,0:T(8,128)(2,1)}) custom-call(f32[8,288,128]{2,1,0:T(8,128)S(1)} %get-tuple-element.57.grad_conv, f32[31,1024]{1,0:T(8,128)S(1)} %copy-done.4, bf16[256,1024]{1,0:T(8,128)(2,1)S(1)} %copy-done.1, ...), custom_call_target="tpu_custom_call", output_to_operand_aliasing={{0}: (0, {}), {1}: (9, {}), {2}: (10, {})} | custom-call | flops 2031616 | tf_op jit(solution)/shard_map/pallas_call | solution.py:29
  43.6 0.7 %shard_map.125 = (f32[31,1024]{1,0:T(8,128)}, f32[8,128]{1,0:T(8,128)}, f32[8,128]{1,0:T(8,128)}) custom-call(bf16[272,128]{1,0:T(8,128)(2,1)S(1)} %shard_map.124.mine, bf16[272,128]{1,0:T(8,128)(2,1)S(1)} %collective-permute-done.9.other), custom_call_target="tpu_custom_call" | custom-call | tf_op jit(solution)/shard_map/pallas_call | solution.py:29
  (18 shorter events, 0.1 us)
Async XLA Ops:
  0.6 6.1 %copy-start.1 = (bf16[256,1024]{1,0:T(8,128)(2,1)S(1)}, bf16[256,1024]{1,0:T(8,128)(2,1)}, u32[]{:S(2)}) copy-start(bf16[256,1024]{1,0:T(8,128)(2,1)} %value.7) | copy-start | bytes 1572868
  0.6 6.1 %copy-start.2 = (bf16[256,1024]{1,0:T(8,128)(2,1)S(1)}, bf16[256,1024]{1,0:T(8,128)(2,1)}, u32[]{:S(2)}) copy-start(bf16[256,1024]{1,0:T(8,128)(2,1)} %gate.7) | copy-start | bytes 1572868
  0.7 6.1 %copy-start.3 = (bf16[256,2048]{1,0:T(8,128)(2,1)S(1)}, bf16[256,2048]{1,0:T(8,128)(2,1)}, u32[]{:S(2)}) copy-start(bf16[256,2048]{1,0:T(8,128)(2,1)} %grads.3) | copy-start | bytes 3145732
  0.7 6.1 %copy-start = (bf16[1024,2048]{1,0:T(8,128)(2,1)S(1)}, bf16[1024,2048]{1,0:T(8,128)(2,1)}, u32[]{:S(2)}) copy-start(bf16[1024,2048]{1,0:T(8,128)(2,1)} %w.3) | copy-start | bytes 12582916
  1.7 7.6 %collective-permute-start = (bf16[16,1024]{1,0:T(8,128)(2,1)S(1)}, bf16[16,1024]{1,0:T(8,128)(2,1)S(1)}, u32[]{:S(2)}, u32[]{:S(2)}) collective-permute-start(bf16[16,1024]{1,0:T(8,128)(2,1)S(1)} %get-tuple-element.38), channel_id=1, source_target_pairs={{0,2},{4,6},{8,10},{12,14},{16,18},{20,22},{24,26},{28,30},{2,0},{... | collective-permute-start | bytes 98312 | tf_op jit(solution)/shard_map/ppermute | solution.py:506
  3.3 4.2 %copy-start.4 = (f32[31,1024]{1,0:T(8,128)S(1)}, f32[31,1024]{1,0:T(8,128)}, u32[]{:S(2)}) copy-start(f32[31,1024]{1,0:T(8,128)} %taps.9) | copy-start | bytes 380932
  3.3 7.7 %collective-permute-start.1 = (bf16[16,1024]{1,0:T(8,128)(2,1)S(1)}, bf16[16,1024]{1,0:T(8,128)(2,1)S(1)}, u32[]{:S(2)}, u32[]{:S(2)}) collective-permute-start(bf16[16,1024]{1,0:T(8,128)(2,1)S(1)} %get-tuple-element.39), channel_id=1, source_target_pairs={{2,4},{6,8},{10,12},{14,16},{18,20},{22,24},{26,28},{4,2},{8,6},{1... | collective-permute-start | bytes 98312 | tf_op jit(solution)/shard_map/ppermute | solution.py:505
  11.7 1.4 %copy-start.5 = (f32[1024]{0:T(1024)S(1)}, f32[1024]{0:T(1024)}, u32[]{:S(2)}) copy-start(f32[1024]{0:T(1024)} %param.10) | copy-start | bytes 12292
  11.7 1.4 %copy-start.6 = (f32[1024]{0:T(1024)S(1)}, f32[1024]{0:T(1024)}, u32[]{:S(2)}) copy-start(f32[1024]{0:T(1024)} %param.11) | copy-start | bytes 12292
  11.7 1.4 %collective-permute-start.2 = (f32[256,128]{1,0:T(8,128)S(1)}, f32[256,128]{1,0:T(8,128)S(1)}, u32[]{:S(2)}, u32[]{:S(2)}) collective-permute-start(f32[256,128]{1,0:T(8,128)S(1)} %get-tuple-element.45.stats), channel_id=1, source_target_pairs={{0,1},{1,0},{2,3},{3,2},{4,5},{5,4},{6,7},{7,6},{8,9},{9,8},{10,11... | collective-permute-start | bytes 393224 | tf_op jit(solution)/shard_map/ppermute | solution.py:446
  13.9 1.4 %collective-permute-start.4 = (f32[128,128]{1,0:T(8,128)S(1)}, f32[128,128]{1,0:T(8,128)S(1)}, u32[]{:S(2)}, u32[]{:S(2)}) collective-permute-start(f32[128,128]{1,0:T(8,128)S(1)} %get-tuple-element.54.second), channel_id=1, source_target_pairs={{0,1},{1,0},{2,3},{3,2},{4,5},{5,4},{6,7},{7,6},{8,9},{9,8},{10,11... | collective-permute-start | bytes 196616 | tf_op jit(solution)/shard_map/ppermute | solution.py:446
  14.8 1.6 %collective-permute-start.3 = (f32[128,128]{1,0:T(8,128)S(1)}, f32[128,128]{1,0:T(8,128)S(1)}, u32[]{:S(2)}, u32[]{:S(2)}) collective-permute-start(f32[128,128]{1,0:T(8,128)S(1)} %get-tuple-element.48.second), channel_id=1, source_target_pairs={{0,1},{1,0},{2,3},{3,2},{4,5},{5,4},{6,7},{7,6},{8,9},{9,8},{10,11... | collective-permute-start | bytes 196616 | tf_op jit(solution)/shard_map/ppermute | solution.py:446
  17.9 4.7 %collective-permute-start.5 = (bf16[400,128]{1,0:T(8,128)(2,1)S(1)}, bf16[400,128]{1,0:T(8,128)(2,1)S(1)}, u32[]{:S(2)}, u32[]{:S(2)}) collective-permute-start(bf16[400,128]{1,0:T(8,128)(2,1)S(1)} %get-tuple-element.58.mine), channel_id=1, source_target_pairs={{0,2},{2,0},{4,6},{6,4},{8,10},{10,8},{12,14},{14,12},{16,18},{18,... | collective-permute-start | bytes 307208 | tf_op jit(solution)/shard_map/ppermute | solution.py:577
  22.6 4.7 %collective-permute-start.6 = (bf16[400,128]{1,0:T(8,128)(2,1)S(1)}, bf16[400,128]{1,0:T(8,128)(2,1)S(1)}, u32[]{:S(2)}, u32[]{:S(2)}) collective-permute-start(bf16[400,128]{1,0:T(8,128)(2,1)S(1)} %shard_map.119.mine), channel_id=1, source_target_pairs={{0,4},{2,6},{4,0},{6,2},{8,12},{10,14},{12,8},{14,10},{16,20},{18,... | collective-permute-start | bytes 307208 | tf_op jit(solution)/shard_map/ppermute | solution.py:577
  27.4 4.4 %collective-permute-start.8 = (bf16[272,128]{1,0:T(8,128)(2,1)S(1)}, bf16[272,128]{1,0:T(8,128)(2,1)S(1)}, u32[]{:S(2)}, u32[]{:S(2)}) collective-permute-start(bf16[272,128]{1,0:T(8,128)(2,1)S(1)} %shard_map.123.mine), channel_id=1, source_target_pairs={{0,8},{2,10},{4,12},{6,14},{8,0},{10,2},{12,4},{14,6},{16,24},{18,... | collective-permute-start | bytes 208904 | tf_op jit(solution)/shard_map/ppermute | solution.py:577
  31.7 11.8 %collective-permute-start.9 = (bf16[272,128]{1,0:T(8,128)(2,1)S(1)}, bf16[272,128]{1,0:T(8,128)(2,1)S(1)}, u32[]{:S(2)}, u32[]{:S(2)}) collective-permute-start(bf16[272,128]{1,0:T(8,128)(2,1)S(1)} %shard_map.124.mine), channel_id=1, source_target_pairs={{0,16},{2,18},{4,20},{6,22},{8,24},{10,26},{12,28},{14,30},{16,0},... | collective-permute-start | bytes 208904 | tf_op jit(solution)/shard_map/ppermute | solution.py:577
  34.4 7.6 %collective-permute-start.7 = (bf16[128,128]{1,0:T(8,128)(2,1)S(1)}, bf16[128,128]{1,0:T(8,128)(2,1)S(1)}, u32[]{:S(2)}, u32[]{:S(2)}) collective-permute-start(bf16[128,128]{1,0:T(8,128)(2,1)S(1)} %get-tuple-element.59), channel_id=1, source_target_pairs={{2,4},{6,8},{10,12},{14,16},{18,20},{22,24},{26,28},{4,2},{8,6},{1... | collective-permute-start | bytes 98312 | tf_op jit(solution)/shard_map/ppermute | solution.py:585

commit v2 on v1

--- a/solution.py
+++ b/solution.py
@@ -226,12 +226,12 @@
     line[:, LANES:] = inv
 
     def body(chunk, carry):
-        rows = pl.ds(pl.multiple_of(chunk * 16, 16), 16)
-        whole = pl.ds(pl.multiple_of(at + chunk * 16, 16), 16)
+        rows = pl.ds(pl.multiple_of(chunk * 32, 32), 32)
+        whole = pl.ds(pl.multiple_of(at + chunk * 32, 32), 32)
         mean_rows = line[rows, :LANES]
         inv_rows = line[rows, LANES:]
-        first = jnp.zeros((16, LANES), F32)
-        other = jnp.zeros((16, LANES), F32)
+        first = jnp.zeros((32, LANES), F32)
+        other = jnp.zeros((32, LANES), F32)
         kept = []
         for block in range(blocks):
             lanes = slice(block * LANES, (block + 1) * LANES)
@@ -247,13 +247,13 @@
             first = first + grad_norm
             other = other + grad_norm * norm
             product = grad_pre * norm
-            kept += [product[:8] + product[8:], grad_pre[:8] + grad_pre[8:]]
+            kept += [fold(product), fold(grad_pre)]
         part[0, rows, :] = first
         part[1, rows, :] = other
         return tuple(old + new for old, new in zip(carry, kept))
 
     zero = tuple(jnp.zeros((8, LANES), F32) for _ in range(2 * blocks))
-    totals = lax.fori_loop(0, height // 16, body, zero)
+    totals = lax.fori_loop(0, height // 32, body, zero)
     for block in range(blocks):
         for which in range(2):
             sums[which, block : block + 1, :] = jnp.sum(totals[2 * block + which], 0, keepdims=True)
@@ -271,6 +271,13 @@
 
 def fold(term):
     return (term[0:8] + term[8:16]) + (term[16:24] + term[24:32])
+
+
+def fold_two(first, second):
+    top = lax.broadcasted_iota(jnp.int32, first.shape, 0) < 4
+    total = jnp.where(top, first, second) + pltpu.roll(jnp.where(top, second, first), 4, 0)
+    total = total + pltpu.roll(total, 2, 0)
+    return total + pltpu.roll(total, 1, 0)
 
 
 def tap_sums(
@@ -315,15 +322,18 @@
                     if 2 * pair + 1 < kernel:
                         odds[index] = odds[index] + fold(odd_rows * high_gap[span, :])
             for index, pair in enumerate(pairs):
-                for tap, total in ((2 * pair, evens[index]), (2 * pair + 1, odds[index])):
-                    if tap < kernel:
-                        total = both[index] + total
-                        tile = pl.ds(pl.multiple_of((base + tap) * 8, 8), 8)
-                        if final:
-                            total = jnp.sum(total + raw_in[tile, :], 0, keepdims=True)
-                            raw[pl.ds(base + tap, 1), :] = total
-                        else:
-                            raw[tile, :] = total
+                tiles = [both[index] + evens[index], both[index] + odds[index]]
+                for which, tile in enumerate(tiles[: kernel - 2 * pair]):
+                    place = pl.ds(pl.multiple_of((base + 2 * pair + which) * 8, 8), 8)
+                    if final:
+                        tiles[which] = tile + raw_in[place, :]
+                    else:
+                        raw[place, :] = tile
+                if final:
+                    halves = fold_two(*tiles)
+                    for which in range(min(2, kernel - 2 * pair)):
+                        row = halves[4 * which + 3 : 4 * which + 4]
+                        raw[pl.ds(base + 2 * pair + which, 1), :] = row
         if final:
             one = pl.ds(block, 1)
             raw[pl.ds(base + kernel, 1), :] = sums_low[0, one, :] + sums_high[0, one, :]

time: 44.4 us -> 44.3 us (level)
  no operation moved by 1% of the time
where the time goes in v2:
time: 44.3 us; the launch traced here: 44.1 us
  waiting for transfers between devices  16 us (36%)
  Pallas kernels  14.8 us (33%)
  starting transfers between devices  12.4 us (28%)
  between operations  0.89 us (2%)
    pallas_call x16, Pallas kernels, call(): pl.pallas_call(body, out_shape=[jax.ShapeDtypeStruct(shape, dtype) for sh...  14.8 us
    ppermute x4, waiting for transfers between devices, exchange(): return lax.ppermute(array, ('sp', 'tp'), pairs)  9.63 us
    ppermute x1, waiting for transfers between devices, shards(): grads_odd = lax.ppermute(send_odd, 'sp', swap_odd)  4.31 us
    ppermute x4, starting transfers between devices, exchange(): return lax.ppermute(array, ('sp', 'tp'), pairs)  3.48 us
    ppermute x1, starting transfers between devices, shards(): from_odd = lax.ppermute(send_odd, 'sp', swap_odd)  3.4 us
    ppermute x1, starting transfers between devices, shards(): grads_odd = lax.ppermute(send_odd, 'sp', swap_odd)  3.27 us
    ppermute x1, waiting for transfers between devices, shards(): from_odd = lax.ppermute(send_odd, 'sp', swap_odd)  1.69 us
    ppermute x1, starting transfers between devices, shards(): from_even = lax.ppermute(send_even, 'sp', swap_even)  1.56 us
  transfers between devices with their start and end apart: 10, of which 6 were waited for; matrix products, arithmetic and copies ran while one was open for 0% of the time, Pallas kernels for 23%

profile of v2, /device:TPU:8, one launch (start us, length us, event | category | flops | bytes accessed | tf_op | source)
XLA Modules:
  0.0 44.1 jit_solution(1840201641532948278)
XLA Ops:
  0.7 1.0 %shard_map.110 = (bf16[16,1024]{1,0:T(8,128)(2,1)S(1)}, bf16[16,1024]{1,0:T(8,128)(2,1)S(1)}) custom-call(bf16[256,1024]{1,0:T(8,128)(2,1)} %value.7, bf16[256,1024]{1,0:T(8,128)(2,1)} %gate.7), custom_call_target="tpu_custom_call" | custom-call | flops 32505856000 | tf_op jit(solution)/shard_map/pallas_call | solution.py:29
  1.7 1.6 %collective-permute-start = (bf16[16,1024]{1,0:T(8,128)(2,1)S(1)}, bf16[16,1024]{1,0:T(8,128)(2,1)S(1)}, u32[]{:S(2)}, u32[]{:S(2)}) collective-permute-start(bf16[16,1024]{1,0:T(8,128)(2,1)S(1)} %get-tuple-element.38), channel_id=1, source_target_pairs={{0,2},{4,6},{8,10},{12,14},{16,18},{20,22},{24,26},{28,30},{2,0},{... | collective-permute-start | bytes 98312 | tf_op jit(solution)/shard_map/ppermute | solution.py:516
  3.3 3.4 %collective-permute-start.1 = (bf16[16,1024]{1,0:T(8,128)(2,1)S(1)}, bf16[16,1024]{1,0:T(8,128)(2,1)S(1)}, u32[]{:S(2)}, u32[]{:S(2)}) collective-permute-start(bf16[16,1024]{1,0:T(8,128)(2,1)S(1)} %get-tuple-element.39), channel_id=1, source_target_pairs={{2,4},{6,8},{10,12},{14,16},{18,20},{22,24},{26,28},{4,2},{8,6},{1... | collective-permute-start | bytes 98312 | tf_op jit(solution)/shard_map/ppermute | solution.py:515
  6.7 0.7 %shard_map.111 = (f32[8,288,128]{2,1,0:T(8,128)S(1)}, f32[2,256,128]{2,1,0:T(8,128)S(1)}) custom-call(bf16[256,1024]{1,0:T(8,128)(2,1)S(1)} %copy-done.1, bf16[256,1024]{1,0:T(8,128)(2,1)S(1)} %copy-done.2, bf16[256,2048]{1,0:T(8,128)(2,1)S(1)} %copy-done.3, bf16[1024,2048]{1,0:T(8,128)(2,1)S(1)} %copy-done), custom_call_target="tpu_custom_call" | custom-call | flops 32505856 | tf_op jit(solution)/shard_map/pallas_call | solution.py:29
  7.5 1.8 %shard_map.112 = (f32[8,256,128]{2,1,0:T(8,128)S(1)}, f32[2,256,128]{2,1,0:T(8,128)S(1)}) custom-call(f32[8,288,128]{2,1,0:T(8,128)S(1)} %get-tuple-element.40.gated.gated_in, f32[31,1024]{1,0:T(8,128)S(1)} %copy-done.4), custom_call_target="tpu_custom_call" | custom-call | flops 16252928 | tf_op jit(solution)/shard_map/pallas_call | solution.py:29
  9.3 1.7 %collective-permute-done.1.from_odd = bf16[16,1024]{1,0:T(8,128)(2,1)S(1)} collective-permute-done((bf16[16,1024]{1,0:T(8,128)(2,1)S(1)}, bf16[16,1024]{1,0:T(8,128)(2,1)S(1)}, u32[]{:S(2)}, u32[]{:S(2)}) %collective-permute-start.1) | collective-permute-done | bytes 32800 | tf_op jit(solution)/shard_map/ppermute | solution.py:515
  11.0 0.7 %shard_map.113 = (f32[8,288,128]{2,1,0:T(8,128)S(1)}, f32[8,256,128]{2,1,0:T(8,128)S(1)}, f32[2,256,128]{2,1,0:T(8,128)S(1)}, f32[256,128]{1,0:T(8,128)S(1)}) custom-call(bf16[16,1024]{1,0:T(8,128)(2,1)S(1)} %collective-permute-done.from_even, ...), custom_call_target="tpu_custom_call", output_to_operand_aliasing={{0}: (3, {}), {1}: (4, {}), {2}: (5, {})} | custom-call | flops 16252928 | tf_op jit(solution)/shard_map/pallas_call | solution.py:29
  11.7 0.0 copy-start.5
  11.7 0.0 copy-start.6
  11.7 0.1 collective-permute-start.2
  11.8 1.0 %shard_map.114.mix_high = f32[6,256,128]{2,1,0:T(8,128)S(1)} custom-call(bf16[256,2048]{1,0:T(8,128)(2,1)S(1)} %copy-done.3, bf16[1024,2048]{1,0:T(8,128)(2,1)S(1)} %copy-done), custom_call_target="tpu_custom_call" | custom-call | flops 16252928 | tf_op jit(solution)/shard_map/pallas_call | solution.py:29
  12.8 0.3 collective-permute-done.2.stats_other
  13.1 0.6 %shard_map.116 = (f32[8,128,128]{2,1,0:T(8,128)S(1)}, f32[8,128,128]{2,1,0:T(8,128)S(1)}, f32[128,128]{1,0:T(8,128)S(1)}, f32[2,8,128]{2,1,0:T(8,128)S(1)}) custom-call(f32[8,256,128]{2,1,0:T(8,128)S(1)} %get-tuple-element.43.conv, f32[2,256,128]{2,1,0:T(8,128)S(1)} %get-tuple-element.44.mix_low, f32[6,256,128]{2,1,0:T(8,128)S(1)} %shard_map.114.mix_high, ...), custom_call_target="tpu_custom_call" | custom-call | flops 8126464 | tf_op jit(solution)/shard_map/pallas_call | solution.py:29
  13.8 0.3 collective-permute-start.4
  14.1 0.6 %shard_map.115 = (f32[8,128,128]{2,1,0:T(8,128)S(1)}, f32[8,128,128]{2,1,0:T(8,128)S(1)}, f32[128,128]{1,0:T(8,128)S(1)}, f32[2,8,128]{2,1,0:T(8,128)S(1)}) custom-call(f32[8,256,128]{2,1,0:T(8,128)S(1)} %get-tuple-element.43.conv, f32[2,256,128]{2,1,0:T(8,128)S(1)} %get-tuple-element.44.mix_low, f32[6,256,128]{2,1,0:T(8,128)S(1)} %shard_map.114.mix_high, ...), custom_call_target="tpu_custom_call" | custom-call | flops 8126464 | tf_op jit(solution)/shard_map/pallas_call | solution.py:29
  14.7 0.4 collective-permute-start.3
  15.1 0.0 collective-permute-done.4.second_other
  15.1 1.2 %shard_map.117 = (f32[8,288,128]{2,1,0:T(8,128)S(1)}, f32[2048,128]{1,0:T(8,128)S(1)}) custom-call(f32[8,128,128]{2,1,0:T(8,128)S(1)} %get-tuple-element.52.normed, f32[8,128,128]{2,1,0:T(8,128)S(1)} %get-tuple-element.53.grad, f32[256,128]{1,0:T(8,128)S(1)} %get-tuple-element.45.stats, f32[256,128]{1,0:T(8,128)S(1)} %collective-permute-done.2.stats_other, ...), custom_call_target="tpu_custom_call" | custom-call | flops 8126464 | tf_op jit(solution)/shard_map/pallas_call | solution.py:29
  16.3 1.4 %shard_map.118 = (f32[8,288,128]{2,1,0:T(8,128)S(1)}, bf16[400,128]{1,0:T(8,128)(2,1)S(1)}, bf16[128,128]{1,0:T(8,128)(2,1)S(1)}) custom-call(f32[8,128,128]{2,1,0:T(8,128)S(1)} %get-tuple-element.46.normed, f32[8,128,128]{2,1,0:T(8,128)S(1)} %get-tuple-element.47.grad, f32[256,128]{1,0:T(8,128)S(1)} %get-tuple-element.45.stats, ...), custom_call_target="tpu_custom_call", output_to_operand_aliasing={{0}: (9, {})} | custom-call | flops 8126464 | tf_op jit(solution)/shard_map/pallas_call | solution.py:29
  17.7 0.1 collective-permute-start.5
  17.8 4.6 %collective-permute-done.5.other.refs_0_ = bf16[400,128]{1,0:T(8,128)(2,1)S(1)} collective-permute-done((bf16[400,128]{1,0:T(8,128)(2,1)S(1)}, bf16[400,128]{1,0:T(8,128)(2,1)S(1)}, u32[]{:S(2)}, u32[]{:S(2)}) %collective-permute-start.5) | collective-permute-done | bytes 102432 | tf_op jit(solution)/shard_map/ppermute | solution.py:587
  22.5 0.7 %collective-permute-start.6 = (bf16[400,128]{1,0:T(8,128)(2,1)S(1)}, bf16[400,128]{1,0:T(8,128)(2,1)S(1)}, u32[]{:S(2)}, u32[]{:S(2)}) collective-permute-start(bf16[400,128]{1,0:T(8,128)(2,1)S(1)} %shard_map.119.mine), channel_id=1, source_target_pairs={{0,4},{2,6},{4,0},{6,2},{8,12},{10,14},{12,8},{14,10},{16,20},{18,... | collective-permute-start | bytes 307208 | tf_op jit(solution)/shard_map/ppermute | solution.py:587
  23.1 1.6 %shard_map.120 = (bf16[112,1024]{1,0:T(8,128)(2,1)S(1)}, bf16[112,1024]{1,0:T(8,128)(2,1)S(1)}) custom-call(f32[8,288,128]{2,1,0:T(8,128)S(1)} %get-tuple-element.57.grad_conv, f32[31,1024]{1,0:T(8,128)S(1)} %copy-done.4, bf16[256,1024]{1,0:T(8,128)(2,1)S(1)} %copy-done.1, bf16[256,1024]{1,0:T(8,128)(2,1)S(1)} %copy-done.2), custom_call_target="tpu_custom_call" | custom-call | flops 8126464 | tf_op jit(solution)/shard_map/pallas_call | solution.py:29
  24.8 2.4 %collective-permute-done.6.refs_1_.other = bf16[400,128]{1,0:T(8,128)(2,1)S(1)} collective-permute-done((bf16[400,128]{1,0:T(8,128)(2,1)S(1)}, bf16[400,128]{1,0:T(8,128)(2,1)S(1)}, u32[]{:S(2)}, u32[]{:S(2)}) %collective-permute-start.6) | collective-permute-done | bytes 102432 | tf_op jit(solution)/shard_map/ppermute | solution.py:587
  27.2 0.1 collective-permute-start.8
  27.3 1.7 %shard_map.121 = (bf16[112,1024]{1,0:T(8,128)(2,1)S(1)}, bf16[112,1024]{1,0:T(8,128)(2,1)S(1)}, bf16[256,1024]{1,0:T(8,128)(2,1)}, bf16[256,1024]{1,0:T(8,128)(2,1)}) custom-call(f32[8,288,128]{2,1,0:T(8,128)S(1)} %get-tuple-element.57.grad_conv, f32[31,1024]{1,0:T(8,128)S(1)} %copy-done.4, bf16[256,1024]{1,0:T(8,128)(2,1)S(1)} %copy-done.1, ...), custom_call_target="tpu_custom_call" | custom-call | flops 8126464 | tf_op jit(solution)/shard_map/pallas_call | solution.py:29
  29.0 2.6 %collective-permute-done.8.other = bf16[272,128]{1,0:T(8,128)(2,1)S(1)} collective-permute-done((bf16[272,128]{1,0:T(8,128)(2,1)S(1)}, bf16[272,128]{1,0:T(8,128)(2,1)S(1)}, u32[]{:S(2)}, u32[]{:S(2)}) %collective-permute-start.8) | collective-permute-done | bytes 69664 | tf_op jit(solution)/shard_map/ppermute | solution.py:587
  31.6 2.6 %collective-permute-start.9 = (bf16[272,128]{1,0:T(8,128)(2,1)S(1)}, bf16[272,128]{1,0:T(8,128)(2,1)S(1)}, u32[]{:S(2)}, u32[]{:S(2)}) collective-permute-start(bf16[272,128]{1,0:T(8,128)(2,1)S(1)} %shard_map.124.mine), channel_id=1, source_target_pairs={{0,16},{2,18},{4,20},{6,22},{8,24},{10,26},{12,28},{14,30},{16,0},... | collective-permute-start | bytes 208904 | tf_op jit(solution)/shard_map/ppermute | solution.py:587
  34.2 3.3 %collective-permute-start.7 = (bf16[128,128]{1,0:T(8,128)(2,1)S(1)}, bf16[128,128]{1,0:T(8,128)(2,1)S(1)}, u32[]{:S(2)}, u32[]{:S(2)}) collective-permute-start(bf16[128,128]{1,0:T(8,128)(2,1)S(1)} %get-tuple-element.59), channel_id=1, source_target_pairs={{2,4},{6,8},{10,12},{14,16},{18,20},{22,24},{26,28},{4,2},{8,6},{1... | collective-permute-start | bytes 98312 | tf_op jit(solution)/shard_map/ppermute | solution.py:595
  37.5 4.3 %collective-permute-done.7.refs_2_ = bf16[128,128]{1,0:T(8,128)(2,1)S(1)} collective-permute-done((bf16[128,128]{1,0:T(8,128)(2,1)S(1)}, bf16[128,128]{1,0:T(8,128)(2,1)S(1)}, u32[]{:S(2)}, u32[]{:S(2)}) %collective-permute-start.7) | collective-permute-done | bytes 32800 | tf_op jit(solution)/shard_map/ppermute | solution.py:595
  41.8 1.6 %shard_map.122 = (f32[8,288,128]{2,1,0:T(8,128)S(1)}, bf16[256,1024]{1,0:T(8,128)(2,1)}, bf16[256,1024]{1,0:T(8,128)(2,1)}) custom-call(f32[8,288,128]{2,1,0:T(8,128)S(1)} %get-tuple-element.57.grad_conv, f32[31,1024]{1,0:T(8,128)S(1)} %copy-done.4, bf16[256,1024]{1,0:T(8,128)(2,1)S(1)} %copy-done.1, ...), custom_call_target="tpu_custom_call", output_to_operand_aliasing={{0}: (0, {}), {1}: (9, {}), {2}: (10, {})} | custom-call | flops 2031616 | tf_op jit(solution)/shard_map/pallas_call | solution.py:29
  43.4 0.7 %shard_map.125 = (f32[31,1024]{1,0:T(8,128)}, f32[8,128]{1,0:T(8,128)}, f32[8,128]{1,0:T(8,128)}) custom-call(bf16[272,128]{1,0:T(8,128)(2,1)S(1)} %shard_map.124.mine, bf16[272,128]{1,0:T(8,128)(2,1)S(1)} %collective-permute-done.9.other), custom_call_target="tpu_custom_call" | custom-call | tf_op jit(solution)/shard_map/pallas_call | solution.py:29
  (18 shorter events, 0.1 us)
Async XLA Ops:
  0.6 6.1 %copy-start.1 = (bf16[256,1024]{1,0:T(8,128)(2,1)S(1)}, bf16[256,1024]{1,0:T(8,128)(2,1)}, u32[]{:S(2)}) copy-start(bf16[256,1024]{1,0:T(8,128)(2,1)} %value.7) | copy-start | bytes 1572868
  0.6 6.1 %copy-start.2 = (bf16[256,1024]{1,0:T(8,128)(2,1)S(1)}, bf16[256,1024]{1,0:T(8,128)(2,1)}, u32[]{:S(2)}) copy-start(bf16[256,1024]{1,0:T(8,128)(2,1)} %gate.7) | copy-start | bytes 1572868
  0.7 6.1 %copy-start.3 = (bf16[256,2048]{1,0:T(8,128)(2,1)S(1)}, bf16[256,2048]{1,0:T(8,128)(2,1)}, u32[]{:S(2)}) copy-start(bf16[256,2048]{1,0:T(8,128)(2,1)} %grads.3) | copy-start | bytes 3145732
  0.7 6.1 %copy-start = (bf16[1024,2048]{1,0:T(8,128)(2,1)S(1)}, bf16[1024,2048]{1,0:T(8,128)(2,1)}, u32[]{:S(2)}) copy-start(bf16[1024,2048]{1,0:T(8,128)(2,1)} %w.3) | copy-start | bytes 12582916
  1.7 7.6 %collective-permute-start = (bf16[16,1024]{1,0:T(8,128)(2,1)S(1)}, bf16[16,1024]{1,0:T(8,128)(2,1)S(1)}, u32[]{:S(2)}, u32[]{:S(2)}) collective-permute-start(bf16[16,1024]{1,0:T(8,128)(2,1)S(1)} %get-tuple-element.38), channel_id=1, source_target_pairs={{0,2},{4,6},{8,10},{12,14},{16,18},{20,22},{24,26},{28,30},{2,0},{... | collective-permute-start | bytes 98312 | tf_op jit(solution)/shard_map/ppermute | solution.py:516
  3.3 4.2 %copy-start.4 = (f32[31,1024]{1,0:T(8,128)S(1)}, f32[31,1024]{1,0:T(8,128)}, u32[]{:S(2)}) copy-start(f32[31,1024]{1,0:T(8,128)} %taps.9) | copy-start | bytes 380932
  3.3 7.7 %collective-permute-start.1 = (bf16[16,1024]{1,0:T(8,128)(2,1)S(1)}, bf16[16,1024]{1,0:T(8,128)(2,1)S(1)}, u32[]{:S(2)}, u32[]{:S(2)}) collective-permute-start(bf16[16,1024]{1,0:T(8,128)(2,1)S(1)} %get-tuple-element.39), channel_id=1, source_target_pairs={{2,4},{6,8},{10,12},{14,16},{18,20},{22,24},{26,28},{4,2},{8,6},{1... | collective-permute-start | bytes 98312 | tf_op jit(solution)/shard_map/ppermute | solution.py:515
  11.7 1.4 %copy-start.5 = (f32[1024]{0:T(1024)S(1)}, f32[1024]{0:T(1024)}, u32[]{:S(2)}) copy-start(f32[1024]{0:T(1024)} %param.10) | copy-start | bytes 12292
  11.7 1.4 %copy-start.6 = (f32[1024]{0:T(1024)S(1)}, f32[1024]{0:T(1024)}, u32[]{:S(2)}) copy-start(f32[1024]{0:T(1024)} %param.11) | copy-start | bytes 12292
  11.7 1.4 %collective-permute-start.2 = (f32[256,128]{1,0:T(8,128)S(1)}, f32[256,128]{1,0:T(8,128)S(1)}, u32[]{:S(2)}, u32[]{:S(2)}) collective-permute-start(f32[256,128]{1,0:T(8,128)S(1)} %get-tuple-element.45.stats), channel_id=1, source_target_pairs={{0,1},{1,0},{2,3},{3,2},{4,5},{5,4},{6,7},{7,6},{8,9},{9,8},{10,11... | collective-permute-start | bytes 393224 | tf_op jit(solution)/shard_map/ppermute | solution.py:456
  13.8 1.3 %collective-permute-start.4 = (f32[128,128]{1,0:T(8,128)S(1)}, f32[128,128]{1,0:T(8,128)S(1)}, u32[]{:S(2)}, u32[]{:S(2)}) collective-permute-start(f32[128,128]{1,0:T(8,128)S(1)} %get-tuple-element.54.second), channel_id=1, source_target_pairs={{0,1},{1,0},{2,3},{3,2},{4,5},{5,4},{6,7},{7,6},{8,9},{9,8},{10,11... | collective-permute-start | bytes 196616 | tf_op jit(solution)/shard_map/ppermute | solution.py:456
  14.7 1.6 %collective-permute-start.3 = (f32[128,128]{1,0:T(8,128)S(1)}, f32[128,128]{1,0:T(8,128)S(1)}, u32[]{:S(2)}, u32[]{:S(2)}) collective-permute-start(f32[128,128]{1,0:T(8,128)S(1)} %get-tuple-element.48.second), channel_id=1, source_target_pairs={{0,1},{1,0},{2,3},{3,2},{4,5},{5,4},{6,7},{7,6},{8,9},{9,8},{10,11... | collective-permute-start | bytes 196616 | tf_op jit(solution)/shard_map/ppermute | solution.py:456
  17.7 4.7 %collective-permute-start.5 = (bf16[400,128]{1,0:T(8,128)(2,1)S(1)}, bf16[400,128]{1,0:T(8,128)(2,1)S(1)}, u32[]{:S(2)}, u32[]{:S(2)}) collective-permute-start(bf16[400,128]{1,0:T(8,128)(2,1)S(1)} %get-tuple-element.58.mine), channel_id=1, source_target_pairs={{0,2},{2,0},{4,6},{6,4},{8,10},{10,8},{12,14},{14,12},{16,18},{18,... | collective-permute-start | bytes 307208 | tf_op jit(solution)/shard_map/ppermute | solution.py:587
  22.5 4.7 %collective-permute-start.6 = (bf16[400,128]{1,0:T(8,128)(2,1)S(1)}, bf16[400,128]{1,0:T(8,128)(2,1)S(1)}, u32[]{:S(2)}, u32[]{:S(2)}) collective-permute-start(bf16[400,128]{1,0:T(8,128)(2,1)S(1)} %shard_map.119.mine), channel_id=1, source_target_pairs={{0,4},{2,6},{4,0},{6,2},{8,12},{10,14},{12,8},{14,10},{16,20},{18,... | collective-permute-start | bytes 307208 | tf_op jit(solution)/shard_map/ppermute | solution.py:587
  27.2 4.4 %collective-permute-start.8 = (bf16[272,128]{1,0:T(8,128)(2,1)S(1)}, bf16[272,128]{1,0:T(8,128)(2,1)S(1)}, u32[]{:S(2)}, u32[]{:S(2)}) collective-permute-start(bf16[272,128]{1,0:T(8,128)(2,1)S(1)} %shard_map.123.mine), channel_id=1, source_target_pairs={{0,8},{2,10},{4,12},{6,14},{8,0},{10,2},{12,4},{14,6},{16,24},{18,... | collective-permute-start | bytes 208904 | tf_op jit(solution)/shard_map/ppermute | solution.py:587
  31.6 11.8 %collective-permute-start.9 = (bf16[272,128]{1,0:T(8,128)(2,1)S(1)}, bf16[272,128]{1,0:T(8,128)(2,1)S(1)}, u32[]{:S(2)}, u32[]{:S(2)}) collective-permute-start(bf16[272,128]{1,0:T(8,128)(2,1)S(1)} %shard_map.124.mine), channel_id=1, source_target_pairs={{0,16},{2,18},{4,20},{6,22},{8,24},{10,26},{12,28},{14,30},{16,0},... | collective-permute-start | bytes 208904 | tf_op jit(solution)/shard_map/ppermute | solution.py:587
  34.2 7.6 %collective-permute-start.7 = (bf16[128,128]{1,0:T(8,128)(2,1)S(1)}, bf16[128,128]{1,0:T(8,128)(2,1)S(1)}, u32[]{:S(2)}, u32[]{:S(2)}) collective-permute-start(bf16[128,128]{1,0:T(8,128)(2,1)S(1)} %get-tuple-element.59), channel_id=1, source_target_pairs={{2,4},{6,8},{10,12},{14,16},{18,20},{22,24},{26,28},{4,2},{8,6},{1... | collective-permute-start | bytes 98312 | tf_op jit(solution)/shard_map/ppermute | solution.py:595

commit v3 on v1

--- a/solution.py
+++ b/solution.py
@@ -226,12 +226,12 @@
     line[:, LANES:] = inv
 
     def body(chunk, carry):
-        rows = pl.ds(pl.multiple_of(chunk * 16, 16), 16)
-        whole = pl.ds(pl.multiple_of(at + chunk * 16, 16), 16)
+        rows = pl.ds(pl.multiple_of(chunk * 32, 32), 32)
+        whole = pl.ds(pl.multiple_of(at + chunk * 32, 32), 32)
         mean_rows = line[rows, :LANES]
         inv_rows = line[rows, LANES:]
-        first = jnp.zeros((16, LANES), F32)
-        other = jnp.zeros((16, LANES), F32)
+        first = jnp.zeros((32, LANES), F32)
+        other = jnp.zeros((32, LANES), F32)
         kept = []
         for block in range(blocks):
             lanes = slice(block * LANES, (block + 1) * LANES)
@@ -247,13 +247,13 @@
             first = first + grad_norm
             other = other + grad_norm * norm
             product = grad_pre * norm
-            kept += [product[:8] + product[8:], grad_pre[:8] + grad_pre[8:]]
+            kept += [fold(product), fold(grad_pre)]
         part[0, rows, :] = first
         part[1, rows, :] = other
         return tuple(old + new for old, new in zip(carry, kept))
 
     zero = tuple(jnp.zeros((8, LANES), F32) for _ in range(2 * blocks))
-    totals = lax.fori_loop(0, height // 16, body, zero)
+    totals = lax.fori_loop(0, height // 32, body, zero)
     for block in range(blocks):
         for which in range(2):
             sums[which, block : block + 1, :] = jnp.sum(totals[2 * block + which], 0, keepdims=True)
@@ -567,7 +567,9 @@
     )
     twos, odds = radices(count)
     cores = lax.axis_size("tp")
-    orders = [twos, twos[1::-1] + twos[:1:-1]]
+    order = twos[:1] + twos[1:3][::-1] + twos[3:]
+    turned = [step for at in range(0, len(order), 2) for step in order[at : at + 2][::-1]]
+    orders = [order, turned]
 
     def exchange(at, array):
         pairs = []

time: 44.4 us -> 44.3 us (level)
  no operation moved by 1% of the time
where the time goes in v3:
time: 44.3 us; the launch traced here: 44.1 us
  waiting for transfers between devices  16 us (36%)
  Pallas kernels  14.8 us (33%)
  starting transfers between devices  12.4 us (28%)
  between operations  0.89 us (2%)
    pallas_call x16, Pallas kernels, call(): pl.pallas_call(body, out_shape=[jax.ShapeDtypeStruct(shape, dtype) for sh...  14.8 us
    ppermute x4, waiting for transfers between devices, exchange(): return lax.ppermute(array, ('sp', 'tp'), pairs)  9.63 us
    ppermute x1, waiting for transfers between devices, shards(): grads_odd = lax.ppermute(send_odd, 'sp', swap_odd)  4.31 us
    ppermute x4, starting transfers between devices, exchange(): return lax.ppermute(array, ('sp', 'tp'), pairs)  3.48 us
    ppermute x1, starting transfers between devices, shards(): from_odd = lax.ppermute(send_odd, 'sp', swap_odd)  3.4 us
    ppermute x1, starting transfers between devices, shards(): grads_odd = lax.ppermute(send_odd, 'sp', swap_odd)  3.27 us
    ppermute x1, waiting for transfers between devices, shards(): from_odd = lax.ppermute(send_odd, 'sp', swap_odd)  1.69 us
    ppermute x1, starting transfers between devices, shards(): from_even = lax.ppermute(send_even, 'sp', swap_even)  1.56 us
  transfers between devices with their start and end apart: 10, of which 6 were waited for; matrix products, arithmetic and copies ran while one was open for 0% of the time, Pallas kernels for 23%

profile of v3, /device:TPU:8, one launch (start us, length us, event | category | flops | bytes accessed | tf_op | source)
XLA Modules:
  0.0 44.1 jit_solution(5197987117886697392)
XLA Ops:
  0.7 1.0 %shard_map.110 = (bf16[16,1024]{1,0:T(8,128)(2,1)S(1)}, bf16[16,1024]{1,0:T(8,128)(2,1)S(1)}) custom-call(bf16[256,1024]{1,0:T(8,128)(2,1)} %value.7, bf16[256,1024]{1,0:T(8,128)(2,1)} %gate.7), custom_call_target="tpu_custom_call" | custom-call | flops 32505856000 | tf_op jit(solution)/shard_map/pallas_call | solution.py:29
  1.7 1.6 %collective-permute-start = (bf16[16,1024]{1,0:T(8,128)(2,1)S(1)}, bf16[16,1024]{1,0:T(8,128)(2,1)S(1)}, u32[]{:S(2)}, u32[]{:S(2)}) collective-permute-start(bf16[16,1024]{1,0:T(8,128)(2,1)S(1)} %get-tuple-element.38), channel_id=1, source_target_pairs={{0,2},{4,6},{8,10},{12,14},{16,18},{20,22},{24,26},{28,30},{2,0},{... | collective-permute-start | bytes 98312 | tf_op jit(solution)/shard_map/ppermute | solution.py:506
  3.3 3.4 %collective-permute-start.1 = (bf16[16,1024]{1,0:T(8,128)(2,1)S(1)}, bf16[16,1024]{1,0:T(8,128)(2,1)S(1)}, u32[]{:S(2)}, u32[]{:S(2)}) collective-permute-start(bf16[16,1024]{1,0:T(8,128)(2,1)S(1)} %get-tuple-element.39), channel_id=1, source_target_pairs={{2,4},{6,8},{10,12},{14,16},{18,20},{22,24},{26,28},{4,2},{8,6},{1... | collective-permute-start | bytes 98312 | tf_op jit(solution)/shard_map/ppermute | solution.py:505
  6.7 0.7 %shard_map.111 = (f32[8,288,128]{2,1,0:T(8,128)S(1)}, f32[2,256,128]{2,1,0:T(8,128)S(1)}) custom-call(bf16[256,1024]{1,0:T(8,128)(2,1)S(1)} %copy-done.1, bf16[256,1024]{1,0:T(8,128)(2,1)S(1)} %copy-done.2, bf16[256,2048]{1,0:T(8,128)(2,1)S(1)} %copy-done.3, bf16[1024,2048]{1,0:T(8,128)(2,1)S(1)} %copy-done), custom_call_target="tpu_custom_call" | custom-call | flops 32505856 | tf_op jit(solution)/shard_map/pallas_call | solution.py:29
  7.5 1.8 %shard_map.112 = (f32[8,256,128]{2,1,0:T(8,128)S(1)}, f32[2,256,128]{2,1,0:T(8,128)S(1)}) custom-call(f32[8,288,128]{2,1,0:T(8,128)S(1)} %get-tuple-element.40.gated.gated_in, f32[31,1024]{1,0:T(8,128)S(1)} %copy-done.4), custom_call_target="tpu_custom_call" | custom-call | flops 16252928 | tf_op jit(solution)/shard_map/pallas_call | solution.py:29
  9.3 1.7 %collective-permute-done.1.from_odd = bf16[16,1024]{1,0:T(8,128)(2,1)S(1)} collective-permute-done((bf16[16,1024]{1,0:T(8,128)(2,1)S(1)}, bf16[16,1024]{1,0:T(8,128)(2,1)S(1)}, u32[]{:S(2)}, u32[]{:S(2)}) %collective-permute-start.1) | collective-permute-done | bytes 32800 | tf_op jit(solution)/shard_map/ppermute | solution.py:505
  11.0 0.7 %shard_map.113 = (f32[8,288,128]{2,1,0:T(8,128)S(1)}, f32[8,256,128]{2,1,0:T(8,128)S(1)}, f32[2,256,128]{2,1,0:T(8,128)S(1)}, f32[256,128]{1,0:T(8,128)S(1)}) custom-call(bf16[16,1024]{1,0:T(8,128)(2,1)S(1)} %collective-permute-done.from_even, ...), custom_call_target="tpu_custom_call", output_to_operand_aliasing={{0}: (3, {}), {1}: (4, {}), {2}: (5, {})} | custom-call | flops 16252928 | tf_op jit(solution)/shard_map/pallas_call | solution.py:29
  11.7 0.0 copy-start.5
  11.7 0.0 copy-start.6
  11.7 0.1 collective-permute-start.2
  11.8 1.0 %shard_map.114.mix_high = f32[6,256,128]{2,1,0:T(8,128)S(1)} custom-call(bf16[256,2048]{1,0:T(8,128)(2,1)S(1)} %copy-done.3, bf16[1024,2048]{1,0:T(8,128)(2,1)S(1)} %copy-done), custom_call_target="tpu_custom_call" | custom-call | flops 16252928 | tf_op jit(solution)/shard_map/pallas_call | solution.py:29
  12.8 0.3 collective-permute-done.2.stats_other
  13.1 0.6 %shard_map.116 = (f32[8,128,128]{2,1,0:T(8,128)S(1)}, f32[8,128,128]{2,1,0:T(8,128)S(1)}, f32[128,128]{1,0:T(8,128)S(1)}, f32[2,8,128]{2,1,0:T(8,128)S(1)}) custom-call(f32[8,256,128]{2,1,0:T(8,128)S(1)} %get-tuple-element.43.conv, f32[2,256,128]{2,1,0:T(8,128)S(1)} %get-tuple-element.44.mix_low, f32[6,256,128]{2,1,0:T(8,128)S(1)} %shard_map.114.mix_high, ...), custom_call_target="tpu_custom_call" | custom-call | flops 8126464 | tf_op jit(solution)/shard_map/pallas_call | solution.py:29
  13.8 0.3 collective-permute-start.4
  14.1 0.6 %shard_map.115 = (f32[8,128,128]{2,1,0:T(8,128)S(1)}, f32[8,128,128]{2,1,0:T(8,128)S(1)}, f32[128,128]{1,0:T(8,128)S(1)}, f32[2,8,128]{2,1,0:T(8,128)S(1)}) custom-call(f32[8,256,128]{2,1,0:T(8,128)S(1)} %get-tuple-element.43.conv, f32[2,256,128]{2,1,0:T(8,128)S(1)} %get-tuple-element.44.mix_low, f32[6,256,128]{2,1,0:T(8,128)S(1)} %shard_map.114.mix_high, ...), custom_call_target="tpu_custom_call" | custom-call | flops 8126464 | tf_op jit(solution)/shard_map/pallas_call | solution.py:29
  14.7 0.4 collective-permute-start.3
  15.1 0.0 collective-permute-done.4.second_other
  15.1 1.2 %shard_map.117 = (f32[8,288,128]{2,1,0:T(8,128)S(1)}, f32[2048,128]{1,0:T(8,128)S(1)}) custom-call(f32[8,128,128]{2,1,0:T(8,128)S(1)} %get-tuple-element.52.normed, f32[8,128,128]{2,1,0:T(8,128)S(1)} %get-tuple-element.53.grad, f32[256,128]{1,0:T(8,128)S(1)} %get-tuple-element.45.stats, f32[256,128]{1,0:T(8,128)S(1)} %collective-permute-done.2.stats_other, ...), custom_call_target="tpu_custom_call" | custom-call | flops 8126464 | tf_op jit(solution)/shard_map/pallas_call | solution.py:29
  16.3 1.4 %shard_map.118 = (f32[8,288,128]{2,1,0:T(8,128)S(1)}, bf16[400,128]{1,0:T(8,128)(2,1)S(1)}, bf16[128,128]{1,0:T(8,128)(2,1)S(1)}) custom-call(f32[8,128,128]{2,1,0:T(8,128)S(1)} %get-tuple-element.46.normed, f32[8,128,128]{2,1,0:T(8,128)S(1)} %get-tuple-element.47.grad, f32[256,128]{1,0:T(8,128)S(1)} %get-tuple-element.45.stats, ...), custom_call_target="tpu_custom_call", output_to_operand_aliasing={{0}: (9, {})} | custom-call | flops 8126464 | tf_op jit(solution)/shard_map/pallas_call | solution.py:29
  17.7 0.1 collective-permute-start.5
  17.8 4.6 %collective-permute-done.5.other.refs_0_ = bf16[400,128]{1,0:T(8,128)(2,1)S(1)} collective-permute-done((bf16[400,128]{1,0:T(8,128)(2,1)S(1)}, bf16[400,128]{1,0:T(8,128)(2,1)S(1)}, u32[]{:S(2)}, u32[]{:S(2)}) %collective-permute-start.5) | collective-permute-done | bytes 102432 | tf_op jit(solution)/shard_map/ppermute | solution.py:579
  22.5 0.1 collective-permute-start.6
  22.6 1.6 %shard_map.120 = (bf16[112,1024]{1,0:T(8,128)(2,1)S(1)}, bf16[112,1024]{1,0:T(8,128)(2,1)S(1)}) custom-call(f32[8,288,128]{2,1,0:T(8,128)S(1)} %get-tuple-element.57.grad_conv, f32[31,1024]{1,0:T(8,128)S(1)} %copy-done.4, bf16[256,1024]{1,0:T(8,128)(2,1)S(1)} %copy-done.1, bf16[256,1024]{1,0:T(8,128)(2,1)S(1)} %copy-done.2), custom_call_target="tpu_custom_call" | custom-call | flops 8126464 | tf_op jit(solution)/shard_map/pallas_call | solution.py:29
  24.2 3.0 %collective-permute-done.6.refs_1_.other = bf16[400,128]{1,0:T(8,128)(2,1)S(1)} collective-permute-done((bf16[400,128]{1,0:T(8,128)(2,1)S(1)}, bf16[400,128]{1,0:T(8,128)(2,1)S(1)}, u32[]{:S(2)}, u32[]{:S(2)}) %collective-permute-start.6) | collective-permute-done | bytes 102432 | tf_op jit(solution)/shard_map/ppermute | solution.py:579
  27.2 0.7 %collective-permute-start.8 = (bf16[272,128]{1,0:T(8,128)(2,1)S(1)}, bf16[272,128]{1,0:T(8,128)(2,1)S(1)}, u32[]{:S(2)}, u32[]{:S(2)}) collective-permute-start(bf16[272,128]{1,0:T(8,128)(2,1)S(1)} %shard_map.123.mine), channel_id=1, source_target_pairs={{0,4},{2,6},{4,0},{6,2},{8,12},{10,14},{12,8},{14,10},{16,20},{18,... | collective-permute-start | bytes 208904 | tf_op jit(solution)/shard_map/ppermute | solution.py:579
  27.9 1.7 %shard_map.121 = (bf16[112,1024]{1,0:T(8,128)(2,1)S(1)}, bf16[112,1024]{1,0:T(8,128)(2,1)S(1)}, bf16[256,1024]{1,0:T(8,128)(2,1)}, bf16[256,1024]{1,0:T(8,128)(2,1)}) custom-call(f32[8,288,128]{2,1,0:T(8,128)S(1)} %get-tuple-element.57.grad_conv, f32[31,1024]{1,0:T(8,128)S(1)} %copy-done.4, bf16[256,1024]{1,0:T(8,128)(2,1)S(1)} %copy-done.1, ...), custom_call_target="tpu_custom_call" | custom-call | flops 8126464 | tf_op jit(solution)/shard_map/pallas_call | solution.py:29
  29.6 2.0 %collective-permute-done.8.other = bf16[272,128]{1,0:T(8,128)(2,1)S(1)} collective-permute-done((bf16[272,128]{1,0:T(8,128)(2,1)S(1)}, bf16[272,128]{1,0:T(8,128)(2,1)S(1)}, u32[]{:S(2)}, u32[]{:S(2)}) %collective-permute-start.8) | collective-permute-done | bytes 69664 | tf_op jit(solution)/shard_map/ppermute | solution.py:579
  31.6 2.6 %collective-permute-start.9 = (bf16[272,128]{1,0:T(8,128)(2,1)S(1)}, bf16[272,128]{1,0:T(8,128)(2,1)S(1)}, u32[]{:S(2)}, u32[]{:S(2)}) collective-permute-start(bf16[272,128]{1,0:T(8,128)(2,1)S(1)} %shard_map.124.mine), channel_id=1, source_target_pairs={{0,16},{2,18},{4,20},{6,22},{8,24},{10,26},{12,28},{14,30},{16,0},... | collective-permute-start | bytes 208904 | tf_op jit(solution)/shard_map/ppermute | solution.py:579
  34.3 3.3 %collective-permute-start.7 = (bf16[128,128]{1,0:T(8,128)(2,1)S(1)}, bf16[128,128]{1,0:T(8,128)(2,1)S(1)}, u32[]{:S(2)}, u32[]{:S(2)}) collective-permute-start(bf16[128,128]{1,0:T(8,128)(2,1)S(1)} %get-tuple-element.59), channel_id=1, source_target_pairs={{2,4},{6,8},{10,12},{14,16},{18,20},{22,24},{26,28},{4,2},{8,6},{1... | collective-permute-start | bytes 98312 | tf_op jit(solution)/shard_map/ppermute | solution.py:587
  37.6 4.3 %collective-permute-done.7.refs_2_ = bf16[128,128]{1,0:T(8,128)(2,1)S(1)} collective-permute-done((bf16[128,128]{1,0:T(8,128)(2,1)S(1)}, bf16[128,128]{1,0:T(8,128)(2,1)S(1)}, u32[]{:S(2)}, u32[]{:S(2)}) %collective-permute-start.7) | collective-permute-done | bytes 32800 | tf_op jit(solution)/shard_map/ppermute | solution.py:587
  41.9 1.6 %shard_map.122 = (f32[8,288,128]{2,1,0:T(8,128)S(1)}, bf16[256,1024]{1,0:T(8,128)(2,1)}, bf16[256,1024]{1,0:T(8,128)(2,1)}) custom-call(f32[8,288,128]{2,1,0:T(8,128)S(1)} %get-tuple-element.57.grad_conv, f32[31,1024]{1,0:T(8,128)S(1)} %copy-done.4, bf16[256,1024]{1,0:T(8,128)(2,1)S(1)} %copy-done.1, ...), custom_call_target="tpu_custom_call", output_to_operand_aliasing={{0}: (0, {}), {1}: (9, {}), {2}: (10, {})} | custom-call | flops 2031616 | tf_op jit(solution)/shard_map/pallas_call | solution.py:29
  43.4 0.7 %shard_map.125 = (f32[31,1024]{1,0:T(8,128)}, f32[8,128]{1,0:T(8,128)}, f32[8,128]{1,0:T(8,128)}) custom-call(bf16[272,128]{1,0:T(8,128)(2,1)S(1)} %shard_map.124.mine, bf16[272,128]{1,0:T(8,128)(2,1)S(1)} %collective-permute-done.9.other), custom_call_target="tpu_custom_call" | custom-call | tf_op jit(solution)/shard_map/pallas_call | solution.py:29
  (18 shorter events, 0.1 us)
Async XLA Ops:
  0.6 6.1 %copy-start.1 = (bf16[256,1024]{1,0:T(8,128)(2,1)S(1)}, bf16[256,1024]{1,0:T(8,128)(2,1)}, u32[]{:S(2)}) copy-start(bf16[256,1024]{1,0:T(8,128)(2,1)} %value.7) | copy-start | bytes 1572868
  0.6 6.1 %copy-start.2 = (bf16[256,1024]{1,0:T(8,128)(2,1)S(1)}, bf16[256,1024]{1,0:T(8,128)(2,1)}, u32[]{:S(2)}) copy-start(bf16[256,1024]{1,0:T(8,128)(2,1)} %gate.7) | copy-start | bytes 1572868
  0.7 6.1 %copy-start.3 = (bf16[256,2048]{1,0:T(8,128)(2,1)S(1)}, bf16[256,2048]{1,0:T(8,128)(2,1)}, u32[]{:S(2)}) copy-start(bf16[256,2048]{1,0:T(8,128)(2,1)} %grads.3) | copy-start | bytes 3145732
  0.7 6.1 %copy-start = (bf16[1024,2048]{1,0:T(8,128)(2,1)S(1)}, bf16[1024,2048]{1,0:T(8,128)(2,1)}, u32[]{:S(2)}) copy-start(bf16[1024,2048]{1,0:T(8,128)(2,1)} %w.3) | copy-start | bytes 12582916
  1.7 7.6 %collective-permute-start = (bf16[16,1024]{1,0:T(8,128)(2,1)S(1)}, bf16[16,1024]{1,0:T(8,128)(2,1)S(1)}, u32[]{:S(2)}, u32[]{:S(2)}) collective-permute-start(bf16[16,1024]{1,0:T(8,128)(2,1)S(1)} %get-tuple-element.38), channel_id=1, source_target_pairs={{0,2},{4,6},{8,10},{12,14},{16,18},{20,22},{24,26},{28,30},{2,0},{... | collective-permute-start | bytes 98312 | tf_op jit(solution)/shard_map/ppermute | solution.py:506
  3.3 4.2 %copy-start.4 = (f32[31,1024]{1,0:T(8,128)S(1)}, f32[31,1024]{1,0:T(8,128)}, u32[]{:S(2)}) copy-start(f32[31,1024]{1,0:T(8,128)} %taps.9) | copy-start | bytes 380932
  3.3 7.7 %collective-permute-start.1 = (bf16[16,1024]{1,0:T(8,128)(2,1)S(1)}, bf16[16,1024]{1,0:T(8,128)(2,1)S(1)}, u32[]{:S(2)}, u32[]{:S(2)}) collective-permute-start(bf16[16,1024]{1,0:T(8,128)(2,1)S(1)} %get-tuple-element.39), channel_id=1, source_target_pairs={{2,4},{6,8},{10,12},{14,16},{18,20},{22,24},{26,28},{4,2},{8,6},{1... | collective-permute-start | bytes 98312 | tf_op jit(solution)/shard_map/ppermute | solution.py:505
  11.7 1.4 %copy-start.5 = (f32[1024]{0:T(1024)S(1)}, f32[1024]{0:T(1024)}, u32[]{:S(2)}) copy-start(f32[1024]{0:T(1024)} %param.10) | copy-start | bytes 12292
  11.7 1.4 %copy-start.6 = (f32[1024]{0:T(1024)S(1)}, f32[1024]{0:T(1024)}, u32[]{:S(2)}) copy-start(f32[1024]{0:T(1024)} %param.11) | copy-start | bytes 12292
  11.7 1.4 %collective-permute-start.2 = (f32[256,128]{1,0:T(8,128)S(1)}, f32[256,128]{1,0:T(8,128)S(1)}, u32[]{:S(2)}, u32[]{:S(2)}) collective-permute-start(f32[256,128]{1,0:T(8,128)S(1)} %get-tuple-element.45.stats), channel_id=1, source_target_pairs={{0,1},{1,0},{2,3},{3,2},{4,5},{5,4},{6,7},{7,6},{8,9},{9,8},{10,11... | collective-permute-start | bytes 393224 | tf_op jit(solution)/shard_map/ppermute | solution.py:446
  13.8 1.3 %collective-permute-start.4 = (f32[128,128]{1,0:T(8,128)S(1)}, f32[128,128]{1,0:T(8,128)S(1)}, u32[]{:S(2)}, u32[]{:S(2)}) collective-permute-start(f32[128,128]{1,0:T(8,128)S(1)} %get-tuple-element.54.second), channel_id=1, source_target_pairs={{0,1},{1,0},{2,3},{3,2},{4,5},{5,4},{6,7},{7,6},{8,9},{9,8},{10,11... | collective-permute-start | bytes 196616 | tf_op jit(solution)/shard_map/ppermute | solution.py:446
  14.7 1.6 %collective-permute-start.3 = (f32[128,128]{1,0:T(8,128)S(1)}, f32[128,128]{1,0:T(8,128)S(1)}, u32[]{:S(2)}, u32[]{:S(2)}) collective-permute-start(f32[128,128]{1,0:T(8,128)S(1)} %get-tuple-element.48.second), channel_id=1, source_target_pairs={{0,1},{1,0},{2,3},{3,2},{4,5},{5,4},{6,7},{7,6},{8,9},{9,8},{10,11... | collective-permute-start | bytes 196616 | tf_op jit(solution)/shard_map/ppermute | solution.py:446
  17.7 4.7 %collective-permute-start.5 = (bf16[400,128]{1,0:T(8,128)(2,1)S(1)}, bf16[400,128]{1,0:T(8,128)(2,1)S(1)}, u32[]{:S(2)}, u32[]{:S(2)}) collective-permute-start(bf16[400,128]{1,0:T(8,128)(2,1)S(1)} %get-tuple-element.58.mine), channel_id=1, source_target_pairs={{0,2},{2,0},{4,6},{6,4},{8,10},{10,8},{12,14},{14,12},{16,18},{18,... | collective-permute-start | bytes 307208 | tf_op jit(solution)/shard_map/ppermute | solution.py:579
  22.5 4.7 %collective-permute-start.6 = (bf16[400,128]{1,0:T(8,128)(2,1)S(1)}, bf16[400,128]{1,0:T(8,128)(2,1)S(1)}, u32[]{:S(2)}, u32[]{:S(2)}) collective-permute-start(bf16[400,128]{1,0:T(8,128)(2,1)S(1)} %shard_map.119.mine), channel_id=1, source_target_pairs={{0,8},{2,10},{4,12},{6,14},{8,0},{10,2},{12,4},{14,6},{16,24},{18,... | collective-permute-start | bytes 307208 | tf_op jit(solution)/shard_map/ppermute | solution.py:579
  27.2 4.4 %collective-permute-start.8 = (bf16[272,128]{1,0:T(8,128)(2,1)S(1)}, bf16[272,128]{1,0:T(8,128)(2,1)S(1)}, u32[]{:S(2)}, u32[]{:S(2)}) collective-permute-start(bf16[272,128]{1,0:T(8,128)(2,1)S(1)} %shard_map.123.mine), channel_id=1, source_target_pairs={{0,4},{2,6},{4,0},{6,2},{8,12},{10,14},{12,8},{14,10},{16,20},{18,... | collective-permute-start | bytes 208904 | tf_op jit(solution)/shard_map/ppermute | solution.py:579
  31.6 11.8 %collective-permute-start.9 = (bf16[272,128]{1,0:T(8,128)(2,1)S(1)}, bf16[272,128]{1,0:T(8,128)(2,1)S(1)}, u32[]{:S(2)}, u32[]{:S(2)}) collective-permute-start(bf16[272,128]{1,0:T(8,128)(2,1)S(1)} %shard_map.124.mine), channel_id=1, source_target_pairs={{0,16},{2,18},{4,20},{6,22},{8,24},{10,26},{12,28},{14,30},{16,0},... | collective-permute-start | bytes 208904 | tf_op jit(solution)/shard_map/ppermute | solution.py:579
  34.3 7.6 %collective-permute-start.7 = (bf16[128,128]{1,0:T(8,128)(2,1)S(1)}, bf16[128,128]{1,0:T(8,128)(2,1)S(1)}, u32[]{:S(2)}, u32[]{:S(2)}) collective-permute-start(bf16[128,128]{1,0:T(8,128)(2,1)S(1)} %get-tuple-element.59), channel_id=1, source_target_pairs={{2,4},{6,8},{10,12},{14,16},{18,20},{22,24},{26,28},{4,2},{8,6},{1... | collective-permute-start | bytes 98312 | tf_op jit(solution)/shard_map/ppermute | solution.py:587
